TPU v7x, 256 devices: a whole 4x4x8 slice. The times are simulated.
256 devices in a mesh: sp: 64 (over z, y, core), tp: 4 (over x).
Axes of the slice: x: 4, y: 4, z: 8, core: 2. Of those that a mesh axis runs over, the one named last changes fastest.
Arguments:
- stream: bfloat16 [24576, 2048], P(('sp', 'tp')), may hold values from -6 to 6
- query_projected: bfloat16 [24576, 1024], P('sp', 'tp'), may hold values from -6 to 6
- key_projected: bfloat16 [24576, 1024], P('sp', 'tp'), may hold values from -6 to 6
- value_projected: bfloat16 [24576, 1024], P('sp', 'tp'), may hold values from -6 to 6
- gate_projected: bfloat16 [24576, 1024], P('sp', 'tp'), may hold values from -6 to 6
- strength_logits: bfloat16 [8, 24576], P('tp', 'sp'), may hold values from -7 to 4
- decay_preactivation: bfloat16 [8, 24576], P('tp', 'sp'), may hold values from -9 to 9
- extra_log_decay: float32 [8, 24576], P('tp', 'sp'), may hold values from -0.7 to 0
- head_decay_rate: float32 [8], P('tp'), may hold values from 0 to 0.1
- head_norm_gain: float32 [128], replicated, may hold values from 0.1 to 1.9
- head_output_matrix: bfloat16 [1024, 2048], P('tp'), may hold values from -0.1875 to 0.1875
- feed_norm_gain: float32 [2048], replicated, may hold values from 0.1 to 1.9
- gate_matrix: bfloat16 [2048, 5632], P('sp', 'tp'), may hold values from -0.125 to 0.125
- up_matrix: bfloat16 [2048, 5632], P('sp', 'tp'), may hold values from -0.125 to 0.125
- down_matrix: bfloat16 [5632, 2048], P('tp', 'sp'), may hold values from -0.078125 to 0.078125
Outputs:
- result: bfloat16 [24576, 2048], P(('sp', 'tp'))
All inputs are finite; a program needn't handle non-finite values.
Results may differ from a plain program's by a relative error of at most 0.015.
Values may be sent and summed in bfloat16 or wider, within the bound.
A program may use at most 128 MiB of HBM per device.

v0:
```python
import jax
import jax.numpy as jnp
from jax import lax
from jax.sharding import Mesh
from jax.sharding import PartitionSpec as P

HEAD = 128
BLOCK = 64
SP = ("sp_0", "sp_1", "sp_2")
SP_TP = ("sp_0", "sp_1", "sp_2", "tp")


PRECISION_FULL = lax.Precision.HIGHEST
EPSILON = 1e-06


def sent_together(arrays, axis, dim, along):
    widths = [a.shape[along] for a in arrays]
    both = jnp.concatenate(arrays, axis=along)
    out = lax.all_gather(both, axis, axis=dim, tiled=True)
    return tuple(jnp.split(out, [sum(widths[:k]) for k in range(1, len(widths))], axis=along))


def neutral_like(value, identity):
    return jax.tree.map(
        lambda a, e: jnp.broadcast_to(jnp.asarray(e, a.dtype), a.shape), value, identity
    )


def entering(value, axes, combine, identity):
    before = start = neutral_like(value, identity)
    subtotal = value
    for axis in reversed(axes):
        size, index = (lax.axis_size(axis), lax.axis_index(axis))
        pieces = jax.tree.map(
            lambda part, kind: lax.all_gather(part.astype(kind), axis),
            subtotal,
            (jnp.bfloat16, jnp.bfloat16),
        )
        inside, subtotal = (start, start)
        for k in range(size):
            passed = k < index
            subtotal = combine(
                subtotal, jax.tree.map(lambda part, own: part[k].astype(own.dtype), pieces, value)
            )
            inside = jax.tree.map(lambda new, old: jnp.where(passed, new, old), subtotal, inside)
        before = combine(inside, before)
    return before


def split_up(value, dim, size):
    before, after = (value.shape[:dim], value.shape[dim + 1 :])
    return jnp.moveaxis(value.reshape(*before, size, -1, *after), dim, 0)


def sent_and_summed(value, axis, dim):
    tiles = split_up(value, dim, lax.axis_size(axis))
    arrived = lax.all_to_all(tiles, axis, split_axis=0, concat_axis=0, tiled=True)
    return arrived.astype(jnp.float32).sum(axis=0)


def copy_for_each(value, axis):
    copies = jnp.broadcast_to(value, (lax.axis_size(axis), *value.shape))
    return lax.all_to_all(copies, axis, split_axis=0, concat_axis=0, tiled=True)


def in_order(tiles, dim):
    tiles = jnp.moveaxis(tiles, 0, dim)
    lengths = tiles.shape
    return tiles.reshape(*lengths[:dim], lengths[dim] * lengths[dim + 1], *lengths[dim + 2 :])


def gather_directly(value, axis, dim):
    tiles = copy_for_each(value, axis)
    return in_order(tiles, dim)


def unit_rows(tensor):
    return tensor * lax.rsqrt(jnp.sum(tensor * tensor, axis=-1, keepdims=True) + EPSILON)


def rms_scale(tensor):
    return tensor * lax.rsqrt(jnp.mean(tensor * tensor, axis=-1, keepdims=True) + EPSILON)


def block_correction(
    unit_queries,
    unit_keys,
    complete_values,
    strength_logits,
    decay_preactivation,
    extra_log_decay,
    head_decay_rate,
):
    head_count, length, head_width = unit_queries.shape
    block_count = length // BLOCK

    def to_blocks(tensor):
        return tensor.reshape((head_count, block_count, BLOCK) + tensor.shape[2:])

    beta_gate = jax.nn.sigmoid(strength_logits.astype(jnp.float32))
    decay_logarithm = (
        -head_decay_rate[:, None] * jax.nn.softplus(decay_preactivation.astype(jnp.float32))
        + extra_log_decay
    )
    query_block = to_blocks(unit_queries)
    key_block = to_blocks(unit_keys)
    value_block = to_blocks(complete_values)
    beta_block = to_blocks(beta_gate)
    cumulative = jnp.cumsum(to_blocks(decay_logarithm), axis=-1)
    causal = jnp.tril(jnp.ones((BLOCK, BLOCK), bool))
    strict = jnp.tril(jnp.ones((BLOCK, BLOCK), bool), -1)
    spread = cumulative[..., :, None] - cumulative[..., None, :]
    damping = jnp.where(causal, jnp.exp(jnp.where(causal, spread, 0.0)), 0.0)
    key_beta = key_block * beta_block[..., None]
    lower_part = jnp.einsum(
        "hnid,hnjd->hnij", key_beta, key_block, precision=PRECISION_FULL
    ) * jnp.where(strict, damping, 0.0)
    system = lower_part + jnp.eye(BLOCK, dtype=jnp.float32)
    right_side = jnp.concatenate(
        [value_block * beta_block[..., None], key_beta * jnp.exp(cumulative)[..., None]], axis=-1
    )
    solved = lax.linalg.triangular_solve(
        system, right_side, left_side=True, lower=True, unit_diagonal=True
    )
    target_values = solved[..., :head_width]
    householder_weights = solved[..., head_width:]
    inner_scores = (
        jnp.einsum("hnid,hnjd->hnij", query_block, key_block, precision=PRECISION_FULL) * damping
    )
    decayed_queries = query_block * jnp.exp(cumulative)[..., None]
    closing_log_decay = cumulative[..., -1:]
    decayed_keys = key_block * jnp.exp(closing_log_decay - cumulative)[..., None]
    return (
        decayed_queries,
        decayed_keys,
        target_values,
        householder_weights,
        inner_scores,
        closing_log_decay,
    )


def compose(earlier, later):
    first_map, first_shift = earlier
    second_map, second_shift = later
    joined_map = jnp.einsum("hij,hjk->hik", second_map, first_map, precision=PRECISION_FULL)
    joined_shift = (
        jnp.einsum("hij,hjk->hik", second_map, first_shift, precision=PRECISION_FULL) + second_shift
    )
    return (joined_map, joined_shift)


def local_recurrence(
    query_projected,
    key_projected,
    value_projected,
    strength_logits,
    decay_preactivation,
    extra_log_decay,
    head_decay_rate,
):
    head_count = strength_logits.shape[0]
    tok_count = strength_logits.shape[1]

    def split_heads(tensor):
        return tensor.reshape(tok_count, head_count, HEAD).transpose(1, 0, 2).astype(jnp.float32)

    unit_queries = unit_rows(split_heads(query_projected)) * HEAD ** (-0.5)
    unit_keys = unit_rows(split_heads(key_projected))
    complete_values = split_heads(value_projected)
    score_terms = block_correction(
        unit_queries,
        unit_keys,
        complete_values,
        strength_logits,
        decay_preactivation,
        extra_log_decay,
        head_decay_rate,
    )
    identity = jnp.broadcast_to(jnp.eye(HEAD, dtype=jnp.float32), (head_count, HEAD, HEAD))

    def advance(carry, items):
        running_state, matrix_product = carry
        (
            decayed_queries,
            decayed_keys,
            target_values,
            householder_weights,
            inner_scores,
            closing_log_decay,
        ) = items
        new_state = target_values - jnp.einsum(
            "fdc,fcj->fdj", householder_weights, running_state, precision=PRECISION_FULL
        )
        layer_output = jnp.einsum(
            "fdc,fcj->fdj", decayed_queries, running_state, precision=PRECISION_FULL
        )
        layer_output = layer_output + jnp.einsum(
            "hij,hjv->hiv", inner_scores, new_state, precision=PRECISION_FULL
        )
        passed_state = decayed_queries - jnp.einsum(
            "hij,hjk->hik", inner_scores, householder_weights, precision=PRECISION_FULL
        )
        decay_span = jnp.einsum(
            "fdc,fcj->fdj", passed_state, matrix_product, precision=PRECISION_FULL
        )
        decay_factor = jnp.exp(closing_log_decay)[:, :, None]
        step_map = decay_factor * identity - jnp.einsum(
            "hik,hij->hkj", decayed_keys, householder_weights, precision=PRECISION_FULL
        )
        running_state = decay_factor * running_state + jnp.einsum(
            "xwp,xws->xps", decayed_keys, new_state, precision=PRECISION_FULL
        )
        matrix_product = jnp.einsum(
            "hij,hjk->hik", step_map, matrix_product, precision=PRECISION_FULL
        )
        return ((running_state, matrix_product), (layer_output, decay_span))

    moved = tuple((jnp.moveaxis(tensor, 1, 0) for tensor in score_terms))
    zeros_state = jnp.zeros((head_count, HEAD, HEAD), jnp.float32)
    (running_state, matrix_product), (block_outputs, decay_spans) = lax.scan(
        advance, (zeros_state, identity), moved
    )

    def merge_blocks(tensor):
        return jnp.moveaxis(tensor, 0, 1).reshape(head_count, tok_count, HEAD)

    return (
        merge_blocks(block_outputs),
        merge_blocks(decay_spans),
        matrix_product,
        running_state,
        identity,
    )


def feed_forward(whole_rows, gate_matrix, up_matrix, down_matrix):
    gate_whole, up_whole = sent_together((gate_matrix, up_matrix), SP, 0, 1)
    gate_total = jnp.dot(whole_rows, gate_whole, preferred_element_type=jnp.float32)
    up_total = jnp.dot(whole_rows, up_whole, preferred_element_type=jnp.float32)
    hidden = (jax.nn.silu(gate_total) * up_total).astype(jnp.bfloat16)
    down_whole = lax.all_gather(down_matrix, SP, axis=1, tiled=True)
    return jnp.dot(hidden, down_whole, preferred_element_type=jnp.float32)


def body(
    stream,
    query_projected,
    key_projected,
    value_projected,
    gate_projected,
    strength_logits,
    decay_preactivation,
    extra_log_decay,
    head_decay_rate,
    head_norm_gain,
    head_output_matrix,
    feed_norm_gain,
    gate_matrix,
    up_matrix,
    down_matrix,
):
    block_outputs, decay_spans, matrix_product, running_state, identity = local_recurrence(
        query_projected,
        key_projected,
        value_projected,
        strength_logits,
        decay_preactivation,
        extra_log_decay,
        head_decay_rate,
    )
    zeros_state = jnp.zeros_like(running_state)
    _, state_inflow = entering(
        (matrix_product, running_state), SP, compose, (identity, zeros_state)
    )
    attention_output = block_outputs + jnp.einsum(
        "qwc,qcn->qwn", decay_spans, state_inflow, precision=PRECISION_FULL
    )
    head_count = attention_output.shape[0]
    tok_count = attention_output.shape[1]
    normed_heads = rms_scale(attention_output) * head_norm_gain
    gated = normed_heads.transpose(1, 0, 2).reshape(tok_count, head_count * HEAD)
    mixed = (gated * jax.nn.silu(gate_projected.astype(jnp.float32))).astype(jnp.bfloat16)
    branch = sent_and_summed(
        jnp.dot(mixed, head_output_matrix, preferred_element_type=jnp.float32).astype(jnp.bfloat16),
        "tp",
        0,
    )
    residual_own = stream.astype(jnp.float32) + branch
    normed_own = (rms_scale(residual_own) * feed_norm_gain).astype(jnp.bfloat16)
    whole_rows = gather_directly(normed_own, "tp", 0)
    ffn_term = feed_forward(whole_rows, gate_matrix, up_matrix, down_matrix)
    ffn_own = sent_and_summed(ffn_term.astype(jnp.bfloat16), "tp", 0)
    return (residual_own + ffn_own).astype(jnp.bfloat16)


def solution(mesh):
    torus = Mesh(mesh.devices.reshape(8, 4, 2, mesh.shape["tp"]), ("sp_0", "sp_1", "sp_2", "tp"))
    in_specs = (
        P(SP_TP, None),
        P(SP, "tp"),
        P(SP, "tp"),
        P(SP, "tp"),
        P(SP, "tp"),
        P("tp", SP),
        P("tp", SP),
        P("tp", SP),
        P("tp"),
        P(),
        P("tp", None),
        P(),
        P(SP, "tp"),
        P(SP, "tp"),
        P("tp", SP),
    )
    out_specs = P(SP_TP, None)
    return jax.shard_map(body, mesh=torus, in_specs=in_specs, out_specs=out_specs, check_vma=False)
```

profile of v0, /device:TPU:32, one launch (start us, length us, event | category | flops | bytes accessed | tf_op | source)
XLA Modules:
  0.0 279.5 jit_solution(3560800641187166354)
XLA Ops:
  6.5 1.7 pad_maximum_fusion
  10.5 1.1 fusion.69
  11.6 1.1 fusion.73
  14.5 1.1 fusion.71
  16.5 59.0 %custom-call.3 = f32[2,6,1,64,64]{3,4,2,1,0:T(8,128)S(1)} custom-call(f32[2,6,1,64,64]{4,3,2,1,0:T(8,128)S(1)} %fusion.54), custom_call_target="InvertDiagBlocksLowerTriangular" | custom-call | tf_op jit(solution)/shard_map/triangular_solve | solution.py:123
  77.8 21.3 %while.17 = (s32[]{:T(128)}, f32[2,128,128]{2,1,0:T(8,128)S(1)}, f32[2,128,128]{2,1,0:T(8,128)S(1)}, f32[6,2,64,128]{3,2,0,1:T(8,128)}, f32[6,2,64,128]{3,2,0,1:...) while((s32[]{:T(128)}, f32[2,128,128]{2,1,0:T(8,128)S(1)}, ...), condition=%wide.region_4.5_spmd.clone, body=%wide.region_3.4_spmd.clone.sunk | while | flops 201605120 | bytes 2758840 | solution.py:222
  80.2 0.9 fusion.239
  83.8 0.9 fusion.239
  90.9 0.9 fusion.239
  94.4 0.9 fusion.239
  98.0 0.9 fusion.239
  99.2 1.9 all-gather
  101.5 1.2 copy.55
  102.7 1.9 all-gather.3
  104.6 12.8 %all-gather.1 = bf16[8,128,128]{2,1,0:T(8,128)(2,1)S(1)} all-gather(bf16[2,128,128]{2,1,0:T(8,128)(2,1)S(1)} %get-tuple-element.186), channel_id=3, replica_groups=mesh['sp_0'=8,'sp_1'=4,'sp_2'=2,'tp'=4] {'sp_1'}, dimensions={0}, use_global_device_ids=true | all-gather | bytes 327680 | tf_op jit(solution)/shard_map/all_gather | solution.py:36
  117.8 12.4 %all-gather.4 = bf16[8,128,128]{2,1,0:T(8,128)(2,1)S(1)} all-gather(bf16[2,128,128]{2,1,0:T(8,128)(2,1)S(1)} %get-tuple-element.190), channel_id=6, replica_groups=mesh['sp_0'=8,'sp_1'=4,'sp_2'=2,'tp'=4] {'sp_1'}, dimensions={0}, use_global_device_ids=true | all-gather | bytes 327680 | tf_op jit(solution)/shard_map/all_gather | solution.py:36
  131.0 28.8 %all-gather.5 = bf16[16,128,128]{2,1,0:T(8,128)(2,1)S(1)} all-gather(bf16[2,128,128]{2,1,0:T(8,128)(2,1)S(1)} %get-tuple-element.192), channel_id=7, replica_groups=mesh['sp_0'=8,'sp_1'=4,'sp_2'=2,'tp'=4] {'sp_0'}, dimensions={0}, use_global_device_ids=true | all-gather | bytes 589824 | tf_op jit(solution)/shard_map/all_gather | solution.py:36
  160.6 26.0 %all-gather.2 = bf16[16,128,128]{2,1,0:T(8,128)(2,1)S(1)} all-gather(bf16[2,128,128]{2,1,0:T(8,128)(2,1)S(1)} %get-tuple-element.188), channel_id=4, replica_groups=mesh['sp_0'=8,'sp_1'=4,'sp_2'=2,'tp'=4] {'sp_0'}, dimensions={0}, use_global_device_ids=true | all-gather | bytes 589824 | tf_op jit(solution)/shard_map/all_gather | solution.py:36
  191.5 26.1 %all_to_all.15 = bf16[4,96,2048]{2,1,0:T(8,128)(2,1)S(1)} all-to-all(bf16[4,96,2048]{2,1,0:T(8,128)(2,1)S(1)} %bitcast.233), channel_id=1, replica_groups=mesh['sp_0'=8,'sp_1'=4,'sp_2'=2,'tp'=4] {'tp'}, dimensions={0} | all-to-all | bytes 3145728 | tf_op jit(solution)/shard_map/all_to_all | solution.py:58
  218.6 16.9 %all_to_all.16 = bf16[4,96,2048]{2,1,0:T(8,128)(2,1)} all-to-all(bf16[4,96,2048]{2,1,0:T(8,128)(2,1)S(1)} %broadcast_in_dim.70), channel_id=1, replica_groups=mesh['sp_0'=8,'sp_1'=4,'sp_2'=2,'tp'=4] {'tp'}, dimensions={0} | all-to-all | bytes 3145728 | tf_op jit(solution)/shard_map/all_to_all | solution.py:64
  235.5 7.1 %fusion.40 = f32[384,1408]{1,0:T(8,128)} fusion(bf16[384,2048]{1,0:T(8,128)(2,1)} %bitcast.230, bf16[2048,2816]{1,0:T(8,128)(2,1)} %all-gather.9.cloned.1.call-done), kind=kOutput, calls=%fused_computation.46 | convolution fusion | flops 2214592512 | bytes 9502720 | tf_op jit(solution)/shard_map/dot_general | solution.py:240
  242.7 11.6 %convolution_convert_fusion = bf16[384,2048]{1,0:T(8,128)(2,1)} fusion(bf16[1408,2048]{0,1:T(8,128)(2,1)} %all-gather.11.cloned.1.call-done, bf16[384,2048]{1,0:T(8,128)(2,1)} %bitcast.231, bf16[2048,2816]{1,0:T(8,128)(2,1)} %all-gather.9.cloned.1.call-done, f32[384,1408]{1,0:T(8,128)} %fusion.40), kind=kOutput, calls=%fused_computation.52 | convolution fusion | flops 4433215488 | bytes 16842752 | tf_op jit(solution)/shard_map/dot_general | solution.py:244
  254.3 17.2 %all_to_all.17 = bf16[4,96,2048]{2,1,0:T(8,128)(2,1)S(1)} all-to-all(bf16[4,96,2048]{2,1,0:T(8,128)(2,1)} %bitcast.232), channel_id=1, replica_groups=mesh['sp_0'=8,'sp_1'=4,'sp_2'=2,'tp'=4] {'tp'}, dimensions={0} | all-to-all | bytes 3145728 | tf_op jit(solution)/shard_map/all_to_all | solution.py:58
  271.8 0.9 add_convert_fusion
  (141 shorter events, 31.9 us)
Async XLA Ops:
  6.5 184.3 %copy-start = (bf16[256,2048]{1,0:T(8,128)(2,1)S(1)}, bf16[256,2048]{1,0:T(8,128)(2,1)}, u32[]{:S(2)}) copy-start(bf16[256,2048]{1,0:T(8,128)(2,1)} %param.27) | copy-start | bytes 3145732
  6.5 68.9 %copy-start.2 = (bf16[384,256]{1,0:T(8,128)(2,1)S(1)}, bf16[384,256]{1,0:T(8,128)(2,1)}, u32[]{:S(2)}) copy-start(bf16[384,256]{1,0:T(8,128)(2,1)} %param.18) | copy-start | bytes 589828
  6.5 69.1 %copy-start.4 = (bf16[384,256]{1,0:T(8,128)(2,1)S(1)}, bf16[384,256]{1,0:T(8,128)(2,1)}, u32[]{:S(2)}) copy-start(bf16[384,256]{1,0:T(8,128)(2,1)} %param.20) | copy-start | bytes 589828
  6.5 229.0 %all-gather.9.cloned.1.call-start = ((), (), s32[]{:S(2)}) async-start(), calls=%async_computation.3 | async-start | bytes 11714560 | tf_op jit(solution)/shard_map/all_gather | solution.py:20
  8.3 234.3 %all-gather.11.cloned.1.call-start = ((), (), s32[]{:S(2)}) async-start(), calls=%async_computation.4 | async-start | bytes 5857280 | tf_op jit(solution)/shard_map/all_gather | solution.py:243
  188.2 1.7 copy-start.3
  188.7 1.8 copy-start.6
  189.3 1.6 copy-start.7
  191.5 26.4 %copy-start.1 = (bf16[96,2048]{1,0:T(8,128)(2,1)S(1)}, bf16[96,2048]{1,0:T(8,128)(2,1)}, u32[]{:S(2)}) copy-start(bf16[96,2048]{1,0:T(8,128)(2,1)} %param.17) | copy-start | bytes 1179652
  217.6 0.7 copy-start.5
Sparse Core Ops, SparseCore 0:
  10.1 91.3 all-gather.8
  104.2 76.9 all-gather.10
where the time goes:
time: 280 us
  blocking collectives  144 us (51%)
  other arithmetic  69.3 us (25%)
  matrix products  48.7 us (17%)
  between operations  13.9 us (5%)
    all_gather x6, blocking collectives, entering(): lax.all_gather(part.astype(kind), axis)  83.7 us
    another operation x2, other arithmetic, block_correction(): lax.linalg.triangular_solve(system, right_side, left_side=True, lower=Tru...  59 us
    all_to_all x2, blocking collectives, sent_and_summed(): lax.all_to_all(tiles, axis, split_axis=0, concat_axis=0, tiled=True)  43.4 us
    all_to_all x1, blocking collectives, copy_for_each(): return lax.all_to_all(copies, axis, split_axis=0, concat_axis=0, tiled=True)  16.9 us
    dot_general x1, matrix products, feed_forward(): return jnp.dot(hidden, down_whole, preferred_element_type=jnp.float32)  11.6 us
    dot_general x1, matrix products, feed_forward(): jnp.dot(whole_rows, gate_whole, preferred_element_type=jnp.float32)  7.1 us
  transfers between devices with their start and end apart: 2, of which 0 were waited for; matrix products, arithmetic and copies ran while one was open for 38% of the time, Pallas kernels for 0%

commit v1 on v0

v1 whole, which is shorter than its diff:
```python
import functools
import jax
import jax.numpy as jnp
from jax import lax
from jax.experimental import pallas as pl
from jax.experimental.pallas import tpu as pltpu
from jax.sharding import Mesh
from jax.sharding import PartitionSpec as P

HEAD = 128
CHUNK = 128
SP = ("sp_0", "sp_1", "sp_2")
SP_TP = ("sp_0", "sp_1", "sp_2", "tp")
EPSILON = 1e-06
F32 = jnp.float32
BF16 = jnp.bfloat16
HIGH = lax.Precision.HIGHEST
MESH = pl.DeviceIdType.MESH


def mm(a, b):
    return jnp.dot(a.astype(BF16), b.astype(BF16), preferred_element_type=F32)


def mm_nt(a, b):
    return lax.dot_general(a, b, (((1,), (1,)), ((), ())), preferred_element_type=F32)


def mm_tn(a, b):
    return lax.dot_general(
        a.astype(BF16), b.astype(BF16), (((0,), (0,)), ((), ())), preferred_element_type=F32
    )


def full(a, b):
    return jnp.dot(a, b, precision=HIGH, preferred_element_type=F32)


def full_nt(a, b):
    return lax.dot_general(
        a, b, (((1,), (1,)), ((), ())), precision=HIGH, preferred_element_type=F32
    )


def silu(x):
    return x / (1.0 + jnp.exp(-x))


def softplus(x):
    return jnp.maximum(x, 0.0) + jnp.log1p(jnp.exp(-jnp.abs(x)))


def unit_lower_inverses(lowers, row, col):
    inverses = []
    for lower in lowers:
        near = jnp.where((row >> 3) == (col >> 3), lower, 0.0)
        inverses.append((near, jnp.where(row == col, 1.0, 0.0) - near))
    squares = [full(d, d) for d, _ in inverses]
    inverses = [x + full(x, s) for (_, x), s in zip(inverses, squares)]
    squares = [full(s, s) for s in squares]
    inverses = [x + full(x, s) for x, s in zip(inverses, squares)]
    for level in (3, 4, 5, 6):
        between = ((row >> (level + 1)) == (col >> (level + 1))) & ((row >> level) != (col >> level))
        parts = [jnp.where(between, lower, 0.0) for lower in lowers]
        parts = [full(p, x) for p, x in zip(parts, inverses)]
        inverses = [x - full(x, p) for p, x in zip(parts, inverses)]
    return inverses


def local_part(
    q_ref, k_ref, v_ref, strength_ref, decay_ref, extra_ref, rate_ref, maps, from_state, from_values
):
    row = lax.broadcasted_iota(jnp.int32, (CHUNK, CHUNK), 0)
    col = lax.broadcasted_iota(jnp.int32, (CHUNK, CHUNK), 1)
    eye = jnp.where(row == col, 1.0, 0.0)
    lower_ones = jnp.where(row >= col, 1.0, 0.0)
    upper_ones = jnp.where(row <= col, 1.0, 0.0)
    padding = jnp.zeros((6, CHUNK), F32)

    def chunk(c, carry):
        span = pl.ds(pl.multiple_of(c * CHUNK, CHUNK), CHUNK)
        logs = -rate_ref[...] * softplus(decay_ref[:, span].astype(F32)) + extra_ref[:, span]
        beta = 1.0 / (1.0 + jnp.exp(-strength_ref[:, span].astype(F32)))
        logs = jnp.concatenate([logs, padding], axis=0)
        beta = jnp.concatenate([beta, padding], axis=0)
        sums_row = full(logs, upper_ones)
        sums_col = full_nt(lower_ones, logs)
        beta_col = full_nt(eye, beta)
        lowers, scores, rights, keys, queries, closings = [], [], [], [], [], []
        for h in range(2):
            cols = slice(h * HEAD, (h + 1) * HEAD)
            k = k_ref[span, cols]
            q = q_ref[span, cols]
            kf, qf, vf = k.astype(F32), q.astype(F32), v_ref[span, cols].astype(F32)
            squares = kf * kf
            k_col = lax.rsqrt(jnp.sum(squares, axis=1, keepdims=True) + EPSILON)
            k_row = lax.rsqrt(full_nt(jnp.ones((8, HEAD), F32), squares)[0:1] + EPSILON)
            q_col = lax.rsqrt(jnp.sum(qf * qf, axis=1, keepdims=True) + EPSILON) * HEAD ** (-0.5)
            s_col, s_row, b_col = sums_col[:, h : h + 1], sums_row[h : h + 1], beta_col[:, h : h + 1]
            closing = s_row[:, CHUNK - 1 :]
            damping = jnp.exp(jnp.minimum(s_col - s_row, 0.0)) * k_row
            lowers.append(jnp.where(row > col, mm_nt(k, k) * damping * (b_col * k_col), 0.0))
            scores.append(jnp.where(row >= col, mm_nt(q, k) * damping * q_col, 0.0))
            opening = jnp.exp(s_col)
            rights.append(
                jnp.concatenate([kf * (b_col * k_col * opening), vf * b_col], axis=1)
            )
            keys.append(kf * (k_col * jnp.exp(closing - s_col)))
            queries.append(qf * (q_col * opening))
            closings.append(jnp.exp(closing) - 1.0)
        inverses = unit_lower_inverses(lowers, row, col)
        solved = [r + mm(x - eye, r) for x, r in zip(inverses, rights)]
        for h in range(2):
            u = c * 2 + h
            change = mm_tn(keys[h], solved[h])
            maps[u, :, :HEAD] = closings[h] * eye - change[:, :HEAD]
            maps[u, :, HEAD:] = change[:, HEAD:]
            out = mm(scores[h], solved[h])
            from_state[u] = (queries[h] - out[:, :HEAD]).astype(BF16)
            from_values[u] = out[:, HEAD:]
        return carry

    lax.fori_loop(0, 3, chunk, 0)


def joined(earlier, later):
    return earlier + later + mm(later[:, :HEAD], earlier)


def carried(state, pair):
    return state + pair[:, HEAD:] + mm(pair[:, :HEAD], state)


def attention_kernel(
    q_ref,
    k_ref,
    v_ref,
    gate_ref,
    strength_ref,
    decay_ref,
    extra_ref,
    rate_ref,
    gain_ref,
    mixed_ref,
    maps,
    from_state,
    from_values,
    totals,
    pair,
    sib,
    chip,
    zin,
    zout,
    hin,
    hout,
    send_sem,
    recv_sem,
):
    z, y, c = lax.axis_index("sp_0"), lax.axis_index("sp_1"), lax.axis_index("sp_2")
    zin[...] = jnp.zeros_like(zin)
    barrier = pltpu.get_barrier_semaphore()
    peers = [{"sp_2": 1 - c}]
    peers += [{"sp_1": lax.rem(y + d, 4)} for d in (1, 2, 3)]
    peers += [{"sp_0": lax.rem(z + d, 8)} for d in (1, 7)]
    for peer in peers:
        pl.semaphore_signal(barrier, inc=1, device_id=peer, device_id_type=MESH)
    pl.semaphore_wait(barrier, len(peers))

    def copy(src, dst, slot, peer):
        return pltpu.make_async_remote_copy(
            src_ref=src,
            dst_ref=dst,
            send_sem=send_sem.at[slot],
            recv_sem=recv_sem.at[slot],
            device_id=peer,
            device_id_type=MESH,
        )

    local_part(
        q_ref, k_ref, v_ref, strength_ref, decay_ref, extra_ref, rate_ref, maps, from_state, from_values
    )
    for h in range(2):
        total = joined(joined(maps[h], maps[2 + h]), maps[4 + h])
        totals[h] = total
        pair[h] = total.astype(BF16)

    to_sib = copy(pair.at[1 - c], sib, 0, {"sp_2": 1 - c})
    to_sib.start()
    to_sib.wait()
    own, other = totals[c], sib[...].astype(F32)
    first = jnp.where(c == 0, own, other)
    second = jnp.where(c == 0, other, own)
    chip[y] = joined(first, second).astype(BF16)

    sends = []
    for d in (1, 2, 3):
        sends.append(copy(chip.at[y], chip.at[y], d, {"sp_1": lax.rem(y + d, 4)}))
        sends[-1].start()
    for d in (1, 2, 3):
        source = lax.rem(y + 4 - d, 4)
        copy(chip.at[source], chip.at[source], d, {"sp_1": lax.rem(y + d, 4)}).wait_recv()
    total = chip[0].astype(F32)
    before = jnp.where(y == 0, 0.0, total)
    for s in (1, 2, 3):
        total = joined(total, chip[s].astype(F32))
        if s < 3:
            before = jnp.where(y > s, total, before)
    for send in sends:
        send.wait_send()

    onward = copy(zout, zin, 4, {"sp_0": lax.rem(z + 1, 8)})

    @pl.when(z > 0)
    def _():
        onward.wait_recv()

    state = zin[...].astype(F32)

    @pl.when(z < 7)
    def _():
        zout[...] = carried(state, total).astype(BF16)
        onward.start()

    state = carried(state, before)
    later = carried(state, first)
    hout[...] = jnp.where(c == 0, later, state).astype(BF16)
    across = copy(hout, hin, 5, {"sp_2": 1 - c})
    across.start()

    def outputs(h, state):
        cols = pl.ds(pl.multiple_of(h * HEAD, HEAD), HEAD)
        for n in range(3):
            u = n * 2 + h
            span = slice(n * CHUNK, (n + 1) * CHUNK)
            out = from_values[u] + mm(from_state[u], state)
            if n < 2:
                state = carried(state, maps[u])
            out = out * lax.rsqrt(jnp.mean(out * out, axis=1, keepdims=True) + EPSILON)
            gated = out * gain_ref[...] * silu(gate_ref[span, cols].astype(F32))
            mixed_ref[span, cols] = gated.astype(BF16)

    outputs(c, jnp.where(c == 0, state, later))
    across.wait()
    outputs(1 - c, hin[...].astype(F32))

    @pl.when(z < 7)
    def _():
        onward.wait_send()


def attention(q, k, v, gate, strength, decay, extra, rate, gain):
    vmem = pl.BlockSpec(memory_space=pltpu.VMEM)
    return pl.pallas_call(
        attention_kernel,
        name="attention",
        out_shape=jax.ShapeDtypeStruct(q.shape, BF16),
        in_specs=[vmem] * 9,
        out_specs=vmem,
        scratch_shapes=[
            pltpu.VMEM((6, HEAD, 2 * HEAD), F32),
            pltpu.VMEM((6, CHUNK, HEAD), BF16),
            pltpu.VMEM((6, CHUNK, HEAD), F32),
            pltpu.VMEM((2, HEAD, 2 * HEAD), F32),
            pltpu.VMEM((2, HEAD, 2 * HEAD), BF16),
            pltpu.VMEM((HEAD, 2 * HEAD), BF16),
            pltpu.VMEM((4, HEAD, 2 * HEAD), BF16),
            pltpu.VMEM((HEAD, HEAD), BF16),
            pltpu.VMEM((HEAD, HEAD), BF16),
            pltpu.VMEM((HEAD, HEAD), BF16),
            pltpu.VMEM((HEAD, HEAD), BF16),
            pltpu.SemaphoreType.DMA((6,)),
            pltpu.SemaphoreType.DMA((6,)),
        ],
        compiler_params=pltpu.CompilerParams(
            collective_id=0, has_side_effects=True, vmem_limit_bytes=40 * 1024 * 1024
        ),
    )(q, k, v, gate, strength, decay, extra, rate[:, None], gain[None, :])


def sent_together(arrays, axis, dim, along):
    widths = [a.shape[along] for a in arrays]
    both = jnp.concatenate(arrays, axis=along)
    out = lax.all_gather(both, axis, axis=dim, tiled=True)
    return tuple(jnp.split(out, [sum(widths[:k]) for k in range(1, len(widths))], axis=along))


def split_up(value, dim, size):
    before, after = (value.shape[:dim], value.shape[dim + 1 :])
    return jnp.moveaxis(value.reshape(*before, size, -1, *after), dim, 0)


def sent_and_summed(value, axis, dim):
    tiles = split_up(value, dim, lax.axis_size(axis))
    arrived = lax.all_to_all(tiles, axis, split_axis=0, concat_axis=0, tiled=True)
    return arrived.astype(jnp.float32).sum(axis=0)


def copy_for_each(value, axis):
    copies = jnp.broadcast_to(value, (lax.axis_size(axis), *value.shape))
    return lax.all_to_all(copies, axis, split_axis=0, concat_axis=0, tiled=True)


def in_order(tiles, dim):
    tiles = jnp.moveaxis(tiles, 0, dim)
    lengths = tiles.shape
    return tiles.reshape(*lengths[:dim], lengths[dim] * lengths[dim + 1], *lengths[dim + 2 :])


def gather_directly(value, axis, dim):
    tiles = copy_for_each(value, axis)
    return in_order(tiles, dim)


def rms_scale(tensor):
    return tensor * lax.rsqrt(jnp.mean(tensor * tensor, axis=-1, keepdims=True) + EPSILON)


def feed_forward(whole_rows, gate_matrix, up_matrix, down_matrix):
    gate_whole, up_whole = sent_together((gate_matrix, up_matrix), SP, 0, 1)
    gate_total = jnp.dot(whole_rows, gate_whole, preferred_element_type=jnp.float32)
    up_total = jnp.dot(whole_rows, up_whole, preferred_element_type=jnp.float32)
    hidden = (jax.nn.silu(gate_total) * up_total).astype(jnp.bfloat16)
    down_whole = lax.all_gather(down_matrix, SP, axis=1, tiled=True)
    return jnp.dot(hidden, down_whole, preferred_element_type=jnp.float32)


def body(
    stream,
    query_projected,
    key_projected,
    value_projected,
    gate_projected,
    strength_logits,
    decay_preactivation,
    extra_log_decay,
    head_decay_rate,
    head_norm_gain,
    head_output_matrix,
    feed_norm_gain,
    gate_matrix,
    up_matrix,
    down_matrix,
):
    mixed = attention(
        query_projected,
        key_projected,
        value_projected,
        gate_projected,
        strength_logits,
        decay_preactivation,
        extra_log_decay,
        head_decay_rate,
        head_norm_gain,
    )
    branch = sent_and_summed(
        jnp.dot(mixed, head_output_matrix, preferred_element_type=jnp.float32).astype(jnp.bfloat16),
        "tp",
        0,
    )
    residual_own = stream.astype(jnp.float32) + branch
    normed_own = (rms_scale(residual_own) * feed_norm_gain).astype(jnp.bfloat16)
    whole_rows = gather_directly(normed_own, "tp", 0)
    ffn_term = feed_forward(whole_rows, gate_matrix, up_matrix, down_matrix)
    ffn_own = sent_and_summed(ffn_term.astype(jnp.bfloat16), "tp", 0)
    return (residual_own + ffn_own).astype(jnp.bfloat16)


def solution(mesh):
    torus = Mesh(mesh.devices.reshape(8, 4, 2, mesh.shape["tp"]), ("sp_0", "sp_1", "sp_2", "tp"))
    in_specs = (
        P(SP_TP, None),
        P(SP, "tp"),
        P(SP, "tp"),
        P(SP, "tp"),
        P(SP, "tp"),
        P("tp", SP),
        P("tp", SP),
        P("tp", SP),
        P("tp"),
        P(),
        P("tp", None),
        P(),
        P(SP, "tp"),
        P(SP, "tp"),
        P("tp", SP),
    )
    out_specs = P(SP_TP, None)
    return jax.shard_map(body, mesh=torus, in_specs=in_specs, out_specs=out_specs, check_vma=False)
```

time: 280 us -> 226 us (0.81)
  the two profiles are of different devices: /device:TPU:32 before, /device:TPU:1 now
where the time goes in v1:
time: 226 us
  waiting for transfers between devices  82.7 us (37%)
  blocking collectives  70.2 us (31%)
  Pallas kernels  29.1 us (13%)
  matrix products  19.3 us (9%)
  between operations  13.5 us (6%)
  local copies, waits for them, and re-layouts  7.55 us (3%)
  other arithmetic  3.47 us (2%)
    all_gather x1, waiting for transfers between devices, feed_forward(): down_whole = lax.all_gather(down_matrix, SP, axis=1, tiled=True)  72.5 us
    all_to_all x2, blocking collectives, sent_and_summed(): lax.all_to_all(tiles, axis, split_axis=0, concat_axis=0, tiled=True)  48 us
    pallas_call x1, Pallas kernels, attention(): pl.pallas_call(attention_kernel, name='attention', out_shape=jax.ShapeDty...  29.1 us
    all_to_all x1, blocking collectives, copy_for_each(): return lax.all_to_all(copies, axis, split_axis=0, concat_axis=0, tiled=True)  22.2 us
    dot_general x1, matrix products, feed_forward(): return jnp.dot(hidden, down_whole, preferred_element_type=jnp.float32)  11.6 us
    all_gather x1, waiting for transfers between devices, sent_together(): out = lax.all_gather(both, axis, axis=dim, tiled=True)  9.44 us
    dot_general x1, matrix products, feed_forward(): jnp.dot(whole_rows, gate_whole, preferred_element_type=jnp.float32)  7.09 us
    unnamed x22, local copies, waits for them, and re-layouts  6.63 us
  transfers between devices with their start and end apart: 2, of which 2 were waited for; matrix products, arithmetic and copies ran while one was open for 4% of the time, Pallas kernels for 13%

profile of v1, /device:TPU:1, one launch (start us, length us, event | category | flops | bytes accessed | tf_op | source)
XLA Modules:
  0.0 225.8 jit_solution(8958973699534013924)
XLA Ops:
  6.5 1.7 pad_maximum_fusion
  8.3 0.7 all-gather.5.cloned.1.call-update
  9.0 0.7 copy.16.rate_ref
  9.8 0.9 copy-done.1
  10.7 0.9 copy-done.2
  11.6 0.9 copy-done.3
  12.6 0.9 copy-done.4
  13.5 0.7 copy-done.5
  14.2 0.7 copy-done.6
  14.8 0.7 copy-done.7
  15.5 0.7 copy-done.8
  16.2 29.1 %attention.1 = bf16[384,256]{1,0:T(8,128)(2,1)S(1)} custom-call(bf16[384,256]{1,0:T(8,128)(2,1)S(1)} %copy-done.1, bf16[384,256]{1,0:T(8,128)(2,1)S(1)} %copy-done.2, bf16[384,256]{1,0:T(8,128)(2,1)S(1)} %copy-done.3, bf16[384,256]{1,0:T(8,128)(2,1)S(1)} %copy-done.4, bf16[2,384]{1,0:T(2,128)(2,1)S(1)} %copy-done.6, bf16[2,384]{1,0:T(2,128)(2,1)S(1)} %copy-done.7, ...), custom_call_target="tpu_custom_call" | custom-call | tf_op jit(solution)/shard_map/attention/pallas_call | solution.py:253
  45.3 0.6 convolution_convert_fusion.1
  45.9 23.8 %all_to_all.15 = bf16[4,96,2048]{2,1,0:T(8,128)(2,1)S(1)} all-to-all(bf16[4,96,2048]{2,1,0:T(8,128)(2,1)S(1)} %bitcast.11), channel_id=1, replica_groups=mesh['sp_0'=8,'sp_1'=4,'sp_2'=2,'tp'=4] {'tp'}, dimensions={0} | all-to-all | bytes 3145728 | tf_op jit(solution)/shard_map/all_to_all | solution.py:294
  69.7 0.3 convert_reduce_fusion.1
  70.1 0.2 copy-done.10
  70.7 22.2 %all_to_all.16 = bf16[4,96,2048]{2,1,0:T(8,128)(2,1)} all-to-all(bf16[4,96,2048]{2,1,0:T(8,128)(2,1)S(1)} %broadcast_in_dim.13), channel_id=1, replica_groups=mesh['sp_0'=8,'sp_1'=4,'sp_2'=2,'tp'=4] {'tp'}, dimensions={0} | all-to-all | bytes 3145728 | tf_op jit(solution)/shard_map/all_to_all | solution.py:300
  92.9 9.4 %all-gather.3.cloned.1.call-done = bf16[2048,2816]{1,0:T(8,128)(2,1)} async-done(((bf16[32,2816]{1,0:T(8,128)(2,1)}), bf16[2048,2816]{1,0:T(8,128)(2,1)}) %all-gather.3.cloned.1.call-update) | async-done | bytes 11534352 | tf_op jit(solution)/shard_map/all_gather | solution.py:283
  102.3 7.1 %fusion.2 = f32[384,1408]{1,0:T(8,128)} fusion(bf16[384,2048]{1,0:T(8,128)(2,1)} %bitcast.12, bf16[2048,2816]{1,0:T(8,128)(2,1)} %all-gather.3.cloned.1.call-done), kind=kOutput, calls=%fused_computation.2 | convolution fusion | flops 2214592512 | bytes 9502720 | tf_op jit(solution)/shard_map/dot_general | solution.py:320
  109.4 72.5 %all-gather.5.cloned.1.call-done = bf16[1408,2048]{0,1:T(8,128)(2,1)} async-done(((bf16[1408,32]{0,1:T(8,128)(2,1)}), bf16[1408,2048]{0,1:T(8,128)(2,1)}) %all-gather.5.cloned.1.call-update) | async-done | bytes 5767184 | tf_op jit(solution)/shard_map/all_gather | solution.py:323
  181.9 11.6 %convolution_convert_fusion = bf16[384,2048]{1,0:T(8,128)(2,1)} fusion(bf16[1408,2048]{0,1:T(8,128)(2,1)} %all-gather.5.cloned.1.call-done, bf16[384,2048]{1,0:T(8,128)(2,1)} %bitcast.13, bf16[2048,2816]{1,0:T(8,128)(2,1)} %all-gather.3.cloned.1.call-done, f32[384,1408]{1,0:T(8,128)} %fusion.2), kind=kOutput, calls=%fused_computation.8 | convolution fusion | flops 4433215488 | bytes 16842752 | tf_op jit(solution)/shard_map/dot_general | solution.py:324
  193.5 24.2 %all_to_all.17 = bf16[4,96,2048]{2,1,0:T(8,128)(2,1)S(1)} all-to-all(bf16[4,96,2048]{2,1,0:T(8,128)(2,1)} %bitcast.14), channel_id=1, replica_groups=mesh['sp_0'=8,'sp_1'=4,'sp_2'=2,'tp'=4] {'tp'}, dimensions={0} | all-to-all | bytes 3145728 | tf_op jit(solution)/shard_map/all_to_all | solution.py:294
  217.8 0.3 convert_reduce_fusion
  218.0 0.9 add_convert_fusion
  (20 shorter events, 0.6 us)
Async XLA Ops:
  6.5 38.8 %copy-start = (bf16[256,2048]{1,0:T(8,128)(2,1)S(1)}, bf16[256,2048]{1,0:T(8,128)(2,1)}, u32[]{:S(2)}) copy-start(bf16[256,2048]{1,0:T(8,128)(2,1)} %param.25) | copy-start | bytes 3145732
  6.5 95.8 %all-gather.3.cloned.1.call-start = ((), (), s32[]{:S(2)}) async-start(), calls=%async_computation.3 | async-start | bytes 11714560 | tf_op jit(solution)/shard_map/all_gather | solution.py:283
  8.3 173.6 %all-gather.5.cloned.1.call-start = ((), (), s32[]{:S(2)}) async-start(), calls=%async_computation.4 | async-start | bytes 5857280 | tf_op jit(solution)/shard_map/all_gather | solution.py:323
  9.8 0.9 copy-start.1
  10.7 0.9 copy-start.2
  11.6 0.9 copy-start.3
  12.5 0.9 copy-start.4
  13.5 0.7 copy-start.5
  14.2 0.7 copy-start.6
  14.8 0.7 copy-start.7
  15.5 0.7 copy-start.8
  45.9 24.0 %copy-start.9 = (bf16[96,2048]{1,0:T(8,128)(2,1)S(1)}, bf16[96,2048]{1,0:T(8,128)(2,1)}, u32[]{:S(2)}) copy-start(bf16[96,2048]{1,0:T(8,128)(2,1)} %param.15) | copy-start | bytes 1179652
  69.7 0.7 copy-start.10
Sparse Core Ops, SparseCore 0:
  10.1 92.1 all-gather.2
  105.0 76.8 all-gather.4

commit v2 on v1

--- a/solution.py
+++ b/solution.py
@@ -68,7 +68,7 @@
 
 
 def local_part(
-    q_ref, k_ref, v_ref, strength_ref, decay_ref, extra_ref, rate_ref, maps, from_state, from_values
+    q_ref, k_ref, v_ref, strength_ref, decay_ref, extra_ref, rate_ref, maps, from_state, from_values, tick
 ):
     row = lax.broadcasted_iota(jnp.int32, (CHUNK, CHUNK), 0)
     col = lax.broadcasted_iota(jnp.int32, (CHUNK, CHUNK), 1)
@@ -118,6 +118,7 @@
             out = mm(scores[h], solved[h])
             from_state[u] = (queries[h] - out[:, :HEAD]).astype(BF16)
             from_values[u] = out[:, HEAD:]
+        tick(c + 1)
         return carry
 
     lax.fori_loop(0, 3, chunk, 0)
@@ -129,6 +130,115 @@
 
 def carried(state, pair):
     return state + pair[:, HEAD:] + mm(pair[:, :HEAD], state)
+
+
+RINGS = ((0, 1, 16), (0, -1, 15), (1, 1, 16), (1, -1, 15))
+PIECES = (
+    ((0, 0), (0, 16), (2, 0)),
+    ((1, 0), (1, 16), (2, 16)),
+)
+PIECE = 16
+
+
+def place_of(cycle, position):
+    run, step = position // 4, position % 4
+    if cycle == 0:
+        return run, (step + 8 - run) % 4
+    return (3 * run + step) % 8, run % 4
+
+
+def positions(z, y):
+    first = 4 * z + (y + z) % 4
+    step = (z + 16 - 3 * y) % 8
+    second = jnp.where(step < 4, 4 * y + step, 4 * (y + 4) + (step + 4) % 8)
+    return first, second
+
+
+class Gather:
+    def __init__(self, z, y, c, shards, wholes, sems):
+        self.c, self.shards, self.wholes = c, shards, wholes
+        self.ring_send, self.sib_send, self.ring_recv, self.sib_recv = sems
+        self.own = positions(z, y)
+        self.here = z * 4 + y
+        self.targets = []
+        for cycle, way, _ in RINGS:
+            to_z, to_y = place_of(cycle, (self.own[cycle] + 32 + way) % 32)
+            self.targets.append({"sp_0": to_z, "sp_1": to_y})
+
+    def block(self, matrix, first, where):
+        return self.wholes[matrix].at[where, self.c, pl.ds(first, PIECE)]
+
+    def onward(self, ring, piece, step, src, where):
+        matrix, first = PIECES[RINGS[ring][0]][piece]
+        return pltpu.make_async_remote_copy(
+            src_ref=src,
+            dst_ref=self.block(matrix, first, where),
+            send_sem=self.ring_send.at[matrix],
+            recv_sem=self.ring_recv.at[ring, piece, step],
+            device_id=self.targets[ring],
+            device_id_type=MESH,
+        )
+
+    def across(self, src, matrix, dst):
+        return pltpu.make_async_remote_copy(
+            src_ref=src,
+            dst_ref=dst,
+            send_sem=self.sib_send.at[matrix],
+            recv_sem=self.sib_recv.at[matrix],
+            device_id={"sp_2": 1 - self.c},
+            device_id_type=MESH,
+        )
+
+    def start(self):
+        for piece in range(3):
+            for ring in range(4):
+                matrix, first = PIECES[RINGS[ring][0]][piece]
+                src = self.shards[matrix].at[pl.ds(first, PIECE)]
+                self.onward(ring, piece, 0, src, self.here).start()
+        for matrix in range(3):
+            self.across(
+                self.shards[matrix], matrix, self.wholes[matrix].at[self.here, self.c]
+            ).start()
+        for matrix in range(3):
+            self.wholes[matrix][self.here, self.c] = self.shards[matrix][...]
+
+    def tick(self, step):
+        for piece in range(3):
+            for ring in range(4):
+                cycle, way, last = RINGS[ring]
+                matrix, first = PIECES[cycle][piece]
+
+                def move():
+                    z, y = place_of(cycle, (self.own[cycle] + 32 - way * step) % 32)
+                    where = z * 4 + y
+                    block = self.block(matrix, first, where)
+                    self.onward(ring, piece, step - 1, block, where).wait_recv()
+
+                    @pl.when(step < last)
+                    def _():
+                        self.onward(ring, piece, step, block, where).start()
+
+                    self.across(block, matrix, block).start()
+
+                if last == 16:
+                    move()
+                else:
+                    pl.when(step <= last)(move)
+
+    def finish(self):
+        for matrix in range(3):
+            sibling = self.wholes[matrix].at[:, 1 - self.c]
+            self.across(sibling, matrix, sibling).wait()
+        for matrix in range(3):
+            most = self.wholes[matrix].at[pl.ds(0, 31), self.c]
+            pltpu.make_async_remote_copy(
+                src_ref=most,
+                dst_ref=most,
+                send_sem=self.ring_send.at[matrix],
+                recv_sem=self.ring_recv.at[0, 0, 0],
+                device_id=self.targets[0],
+                device_id_type=MESH,
+            ).wait_send()
 
 
 def attention_kernel(
@@ -141,7 +251,13 @@
     extra_ref,
     rate_ref,
     gain_ref,
+    gate_shard,
+    up_shard,
+    down_shard,
     mixed_ref,
+    gate_whole,
+    up_whole,
+    down_whole,
     maps,
     from_state,
     from_values,
@@ -149,22 +265,41 @@
     pair,
     sib,
     chip,
-    zin,
-    zout,
+    zin1,
+    zin2,
+    zin4,
+    zout1,
+    zout2,
+    zout4,
     hin,
     hout,
     send_sem,
     recv_sem,
+    ring_send,
+    sib_send,
+    ring_recv,
+    sib_recv,
 ):
     z, y, c = lax.axis_index("sp_0"), lax.axis_index("sp_1"), lax.axis_index("sp_2")
-    zin[...] = jnp.zeros_like(zin)
+    for ref in (zin1, zin2, zin4):
+        ref[...] = jnp.zeros_like(ref)
     barrier = pltpu.get_barrier_semaphore()
     peers = [{"sp_2": 1 - c}]
     peers += [{"sp_1": lax.rem(y + d, 4)} for d in (1, 2, 3)]
-    peers += [{"sp_0": lax.rem(z + d, 8)} for d in (1, 7)]
+    peers += [{"sp_0": lax.rem(z + d, 8)} for d in (1, 2, 4, 6, 7)]
     for peer in peers:
         pl.semaphore_signal(barrier, inc=1, device_id=peer, device_id_type=MESH)
     pl.semaphore_wait(barrier, len(peers))
+
+    gather = Gather(
+        z,
+        y,
+        c,
+        (gate_shard, up_shard, down_shard),
+        (gate_whole, up_whole, down_whole),
+        (ring_send, sib_send, ring_recv, sib_recv),
+    )
+    gather.start()
 
     def copy(src, dst, slot, peer):
         return pltpu.make_async_remote_copy(
@@ -177,7 +312,17 @@
         )
 
     local_part(
-        q_ref, k_ref, v_ref, strength_ref, decay_ref, extra_ref, rate_ref, maps, from_state, from_values
+        q_ref,
+        k_ref,
+        v_ref,
+        strength_ref,
+        decay_ref,
+        extra_ref,
+        rate_ref,
+        maps,
+        from_state,
+        from_values,
+        gather.tick,
     )
     for h in range(2):
         total = joined(joined(maps[h], maps[2 + h]), maps[4 + h])
@@ -189,13 +334,14 @@
     to_sib.wait()
     own, other = totals[c], sib[...].astype(F32)
     first = jnp.where(c == 0, own, other)
-    second = jnp.where(c == 0, other, own)
-    chip[y] = joined(first, second).astype(BF16)
+    chip[y] = joined(first, jnp.where(c == 0, other, own)).astype(BF16)
+    totals[1] = first
 
     sends = []
     for d in (1, 2, 3):
         sends.append(copy(chip.at[y], chip.at[y], d, {"sp_1": lax.rem(y + d, 4)}))
         sends[-1].start()
+    gather.tick(4)
     for d in (1, 2, 3):
         source = lax.rem(y + 4 - d, 4)
         copy(chip.at[source], chip.at[source], d, {"sp_1": lax.rem(y + d, 4)}).wait_recv()
@@ -208,23 +354,38 @@
     for send in sends:
         send.wait_send()
 
-    onward = copy(zout, zin, 4, {"sp_0": lax.rem(z + 1, 8)})
-
-    @pl.when(z > 0)
-    def _():
-        onward.wait_recv()
-
-    state = zin[...].astype(F32)
-
-    @pl.when(z < 7)
-    def _():
-        zout[...] = carried(state, total).astype(BF16)
-        onward.start()
-
-    state = carried(state, before)
-    later = carried(state, first)
+    totals[0] = before
+    earlier = jnp.zeros((HEAD, 2 * HEAD), F32)
+    hops = ((1, zout1, zin1), (2, zout2, zin2), (4, zout4, zin4))
+    for n, (d, out, arrived) in enumerate(hops):
+        out[...] = total[:, (2 * HEAD - out.shape[1]) :].astype(BF16)
+        hop = copy(out, arrived, 4 + n, {"sp_0": lax.rem(z + d, 8)})
+
+        @pl.when(z + d < 8)
+        def _():
+            hop.start()
+
+        gather.tick(5 + n)
+
+        @pl.when(z >= d)
+        def _():
+            hop.wait_recv()
+
+        came = arrived[...].astype(F32)
+        if d < 4:
+            earlier = joined(came, earlier)
+            total = joined(came, total)
+        else:
+            state = carried(came, earlier)
+
+        @pl.when(z + d < 8)
+        def _():
+            hop.wait_send()
+
+    state = carried(state, totals[0])
+    later = carried(state, totals[1])
     hout[...] = jnp.where(c == 0, later, state).astype(BF16)
-    across = copy(hout, hin, 5, {"sp_2": 1 - c})
+    across = copy(hout, hin, 7, {"sp_2": 1 - c})
     across.start()
 
     def outputs(h, state):
@@ -243,19 +404,23 @@
     across.wait()
     outputs(1 - c, hin[...].astype(F32))
 
-    @pl.when(z < 7)
-    def _():
-        onward.wait_send()
-
-
-def attention(q, k, v, gate, strength, decay, extra, rate, gain):
+    def rest(step, carry):
+        gather.tick(step)
+        return carry
+
+    lax.fori_loop(8, 17, rest, 0)
+    gather.finish()
+
+
+def attention(q, k, v, gate, strength, decay, extra, rate, gain, gate_shard, up_shard, down_shard):
     vmem = pl.BlockSpec(memory_space=pltpu.VMEM)
-    return pl.pallas_call(
+    whole = jax.ShapeDtypeStruct((32, 2, *gate_shard.shape), BF16)
+    mixed, *wholes = pl.pallas_call(
         attention_kernel,
         name="attention",
-        out_shape=jax.ShapeDtypeStruct(q.shape, BF16),
-        in_specs=[vmem] * 9,
-        out_specs=vmem,
+        out_shape=[jax.ShapeDtypeStruct(q.shape, BF16)] + [whole] * 3,
+        in_specs=[vmem] * 12,
+        out_specs=[vmem] * 4,
         scratch_shapes=[
             pltpu.VMEM((6, HEAD, 2 * HEAD), F32),
             pltpu.VMEM((6, CHUNK, HEAD), BF16),
@@ -264,24 +429,26 @@
             pltpu.VMEM((2, HEAD, 2 * HEAD), BF16),
             pltpu.VMEM((HEAD, 2 * HEAD), BF16),
             pltpu.VMEM((4, HEAD, 2 * HEAD), BF16),
+            pltpu.VMEM((HEAD, 2 * HEAD), BF16),
+            pltpu.VMEM((HEAD, 2 * HEAD), BF16),
+            pltpu.VMEM((HEAD, HEAD), BF16),
+            pltpu.VMEM((HEAD, 2 * HEAD), BF16),
+            pltpu.VMEM((HEAD, 2 * HEAD), BF16),
             pltpu.VMEM((HEAD, HEAD), BF16),
             pltpu.VMEM((HEAD, HEAD), BF16),
             pltpu.VMEM((HEAD, HEAD), BF16),
-            pltpu.VMEM((HEAD, HEAD), BF16),
-            pltpu.SemaphoreType.DMA((6,)),
-            pltpu.SemaphoreType.DMA((6,)),
+            pltpu.SemaphoreType.DMA((8,)),
+            pltpu.SemaphoreType.DMA((8,)),
+            pltpu.SemaphoreType.DMA((3,)),
+            pltpu.SemaphoreType.DMA((3,)),
+            pltpu.SemaphoreType.DMA((4, 3, 16)),
+            pltpu.SemaphoreType.DMA((3,)),
         ],
         compiler_params=pltpu.CompilerParams(
-            collective_id=0, has_side_effects=True, vmem_limit_bytes=40 * 1024 * 1024
+            collective_id=0, has_side_effects=True, vmem_limit_bytes=56 * 1024 * 1024
         ),
-    )(q, k, v, gate, strength, decay, extra, rate[:, None], gain[None, :])
-
-
-def sent_together(arrays, axis, dim, along):
-    widths = [a.shape[along] for a in arrays]
-    both = jnp.concatenate(arrays, axis=along)
-    out = lax.all_gather(both, axis, axis=dim, tiled=True)
-    return tuple(jnp.split(out, [sum(widths[:k]) for k in range(1, len(widths))], axis=along))
+    )(q, k, v, gate, strength, decay, extra, rate[:, None], gain[None, :], gate_shard, up_shard, down_shard)
+    return mixed, *(w.reshape(-1, w.shape[-1]) for w in wholes)
 
 
 def split_up(value, dim, size):
@@ -315,13 +482,11 @@
     return tensor * lax.rsqrt(jnp.mean(tensor * tensor, axis=-1, keepdims=True) + EPSILON)
 
 
-def feed_forward(whole_rows, gate_matrix, up_matrix, down_matrix):
-    gate_whole, up_whole = sent_together((gate_matrix, up_matrix), SP, 0, 1)
+def feed_forward(whole_rows, gate_whole, up_whole, down_whole):
     gate_total = jnp.dot(whole_rows, gate_whole, preferred_element_type=jnp.float32)
     up_total = jnp.dot(whole_rows, up_whole, preferred_element_type=jnp.float32)
     hidden = (jax.nn.silu(gate_total) * up_total).astype(jnp.bfloat16)
-    down_whole = lax.all_gather(down_matrix, SP, axis=1, tiled=True)
-    return jnp.dot(hidden, down_whole, preferred_element_type=jnp.float32)
+    return lax.dot_general(hidden, down_whole, (((1,), (1,)), ((), ())), preferred_element_type=jnp.float32)
 
 
 def body(
@@ -341,7 +506,7 @@
     up_matrix,
     down_matrix,
 ):
-    mixed = attention(
+    mixed, gate_whole, up_whole, down_whole = attention(
         query_projected,
         key_projected,
         value_projected,
@@ -351,6 +516,9 @@
         extra_log_decay,
         head_decay_rate,
         head_norm_gain,
+        gate_matrix,
+        up_matrix,
+        down_matrix.T,
     )
     branch = sent_and_summed(
         jnp.dot(mixed, head_output_matrix, preferred_element_type=jnp.float32).astype(jnp.bfloat16),
@@ -360,7 +528,7 @@
     residual_own = stream.astype(jnp.float32) + branch
     normed_own = (rms_scale(residual_own) * feed_norm_gain).astype(jnp.bfloat16)
     whole_rows = gather_directly(normed_own, "tp", 0)
-    ffn_term = feed_forward(whole_rows, gate_matrix, up_matrix, down_matrix)
+    ffn_term = feed_forward(whole_rows, gate_whole, up_whole, down_whole)
     ffn_own = sent_and_summed(ffn_term.astype(jnp.bfloat16), "tp", 0)
     return (residual_own + ffn_own).astype(jnp.bfloat16)
 

time: 226 us -> 181 us (0.80)
  waiting for transfers between devices: 82.7 us -> 0 us
  Pallas kernels: 29.1 us -> 90.8 us
  between operations: 13.5 us -> 0.08 us
  local copies, waits for them, and re-layouts: 7.55 us -> 1.8 us
  blocking collectives: 70.2 us -> 67.9 us
    all_gather x2 -> x0, waiting for transfers between devices: 82 us -> none  [the longest x1 72.5 us: feed_forward(): down_whole = lax.all_gather(down_matrix, SP, axis=1, tiled=True)]
    pallas_call x1, Pallas kernels: 29.1 us -> 90.8 us  [attention(): pl.pallas_call(attention_kernel, name='attention', out_shape=[jax.ShapeDt...]
    unnamed x22 -> x12, local copies, waits for them, and re-layouts: 6.63 us -> 0.23 us
    dot_general x1, matrix products: 7.09 us -> 4.05 us  [feed_forward(): jnp.dot(whole_rows, gate_whole, preferred_element_type=jnp.float32)]
  transfers between devices with their start and end apart: 2 -> 0, of which waited for: 2 -> 0; matrix products, arithmetic and copies ran while one was open for 4% -> 0% of each run, Pallas kernels for 13% -> 0%
where the time goes in v2:
time: 181 us; the launch traced here: 180 us
  Pallas kernels  90.8 us (50%)
  blocking collectives  67.9 us (38%)
  matrix products  17.3 us (10%)
    pallas_call x1, Pallas kernels, attention(): pl.pallas_call(attention_kernel, name='attention', out_shape=[jax.ShapeDt...  90.8 us
    all_to_all x2, blocking collectives, sent_and_summed(): lax.all_to_all(tiles, axis, split_axis=0, concat_axis=0, tiled=True)  46.2 us
    all_to_all x1, blocking collectives, copy_for_each(): return lax.all_to_all(copies, axis, split_axis=0, concat_axis=0, tiled=True)  21.7 us
    dot_general x1, matrix products, feed_forward(): lax.dot_general(hidden, down_whole, (((1,), (1,)), ((), ())), preferred_e...  11.6 us
    dot_general x1, matrix products, feed_forward(): jnp.dot(whole_rows, gate_whole, preferred_element_type=jnp.float32)  4.05 us

profile of v2, /device:TPU:1, one launch (start us, length us, event | category | flops | bytes accessed | tf_op | source)
XLA Modules:
  0.0 179.6 jit_solution(7194700466011634553)
XLA Ops:
  0.0 0.0 copy-start
  0.0 1.4 copy.16.rate_ref
  1.4 90.8 %attention.1 = (bf16[384,256]{1,0:T(8,128)(2,1)}, bf16[32,2,32,1408]{3,2,1,0:T(8,128)(2,1)}, bf16[32,2,32,1408]{3,2,1,0:T(8,128)(2,1)}, bf16[32,2,32,1408]{3,2,1,0:T(8,128)(2,1)}) custom-call(bf16[384,256]{1,0:T(8,128)(2,1)} %q_ref.1, bf16[384,256]{1,0:T(8,128)(2,1)} %k_ref.1, bf16[384,256]{1,0:T(8,128)(2,1)} %v_ref.1, bf16[384,256]{1,0:T(8,128)(2,1)} %gate_ref.1, ...), custom_call_target="tpu_custom_call" | custom-call | tf_op jit(solution)/shard_map/attention/pallas_call | solution.py:418
  92.1 0.0 copy-done
  92.2 0.0 slice-start
  92.2 1.7 convolution_convert_fusion.1
  93.8 0.0 copy-start.1
  93.8 24.3 %all_to_all.15 = bf16[4,96,2048]{2,1,0:T(8,128)(2,1)S(1)} all-to-all(bf16[4,96,2048]{2,1,0:T(8,128)(2,1)S(1)} %bitcast.16), channel_id=1, replica_groups=mesh['sp_0'=8,'sp_1'=4,'sp_2'=2,'tp'=4] {'tp'}, dimensions={0} | all-to-all | bytes 3145728 | tf_op jit(solution)/shard_map/all_to_all | solution.py:461
  118.1 0.0 copy-start.3
  118.1 0.3 convert_reduce_fusion.1
  118.4 0.0 copy-done.1
  118.4 0.2 multiply_reduce_fusion
  118.6 0.2 copy-done.3
  118.8 0.1 multiply_convert_fusion
  119.0 0.2 broadcast_in_dim.13
  119.2 21.7 %all_to_all.16 = bf16[4,96,2048]{2,1,0:T(8,128)(2,1)S(1)} all-to-all(bf16[4,96,2048]{2,1,0:T(8,128)(2,1)S(1)} %broadcast_in_dim.13), channel_id=1, replica_groups=mesh['sp_0'=8,'sp_1'=4,'sp_2'=2,'tp'=4] {'tp'}, dimensions={0} | all-to-all | bytes 3145728 | tf_op jit(solution)/shard_map/all_to_all | solution.py:467
  140.8 0.0 slice-done
  140.8 0.0 slice-done.1
  140.8 4.1 %fusion.2 = f32[384,1408]{1,0:T(8,128)} fusion(bf16[384,2048]{1,0:T(8,128)(2,1)S(1)} %bitcast.17, bf16[2048,1408]{1,0:T(8,128)(2,1)S(1)} %bitcast.26), kind=kOutput, calls=%fused_computation.12 | convolution fusion | flops 2214592512 | bytes 9502720 | tf_op jit(solution)/shard_map/dot_general | solution.py:486
  144.9 0.0 copy-done.2
  144.9 11.6 %convolution_convert_fusion = bf16[384,2048]{1,0:T(8,128)(2,1)} fusion(bf16[2048,1408]{1,0:T(8,128)(2,1)} %bitcast.23, bf16[384,2048]{1,0:T(8,128)(2,1)} %bitcast.18, bf16[2048,1408]{1,0:T(8,128)(2,1)} %bitcast.22, f32[384,1408]{1,0:T(8,128)} %fusion.2), kind=kOutput, calls=%fused_computation.4 | convolution fusion | flops 4433215488 | bytes 16842752 | tf_op jit(solution)/shard_map/dot_general | solution.py:489
  156.5 21.9 %all_to_all.17 = bf16[4,96,2048]{2,1,0:T(8,128)(2,1)S(1)} all-to-all(bf16[4,96,2048]{2,1,0:T(8,128)(2,1)} %bitcast.19), channel_id=1, replica_groups=mesh['sp_0'=8,'sp_1'=4,'sp_2'=2,'tp'=4] {'tp'}, dimensions={0} | all-to-all | bytes 3145728 | tf_op jit(solution)/shard_map/all_to_all | solution.py:461
  178.4 0.3 convert_reduce_fusion
  178.7 0.9 add_convert_fusion
  (4 shorter events, 0.0 us)
Async XLA Ops:
  0.0 92.2 %copy-start = (bf16[256,2048]{1,0:T(8,128)(2,1)S(1)}, bf16[256,2048]{1,0:T(8,128)(2,1)}, u32[]{:S(2)}) copy-start(bf16[256,2048]{1,0:T(8,128)(2,1)} %param.25) | copy-start | bytes 3145732
  92.2 48.7 %slice-start = ((s8[5767168]{0:T(1024)(128)(4,1)}), s8[4194304]{0:T(1024)(128)(4,1)S(1)}, s32[]{:S(2)}) async-start(s8[5767168]{0:T(1024)(128)(4,1)} %bitcast.24), calls=%async_computation.3 | async-start | bytes 8388608
  93.8 24.6 %copy-start.1 = (bf16[96,2048]{1,0:T(8,128)(2,1)S(1)}, bf16[96,2048]{1,0:T(8,128)(2,1)}, u32[]{:S(2)}) copy-start(bf16[96,2048]{1,0:T(8,128)(2,1)} %param.15) | copy-start | bytes 1179652
  118.1 0.7 copy-start.3
  118.1 22.7 %slice-start.1 = ((s8[5767168]{0:T(1024)(128)(4,1)}), s8[1572864]{0:T(1024)(128)(4,1)S(1)}, s32[]{:S(2)}) async-start(s8[5767168]{0:T(1024)(128)(4,1)} %bitcast.24), calls=%async_computation.4 | async-start | bytes 3145728
  140.8 4.1 %copy-start.2 = (bf16[4,96,2048]{2,1,0:T(8,128)(2,1)}, bf16[4,96,2048]{2,1,0:T(8,128)(2,1)S(1)}, u32[]{:S(2)}) copy-start(bf16[4,96,2048]{2,1,0:T(8,128)(2,1)S(1)} %all_to_all.16) | copy-start | bytes 4718596

commit v3 on v1

v3 whole, which is shorter than its diff:
```python
import functools
import jax
import jax.numpy as jnp
from jax import lax
from jax.experimental import pallas as pl
from jax.experimental.pallas import tpu as pltpu
from jax.sharding import Mesh
from jax.sharding import PartitionSpec as P

HEAD = 128
CHUNK = 128
SP = ("sp_0", "sp_1", "sp_2")
SP_TP = ("sp_0", "sp_1", "sp_2", "tp")
EPSILON = 1e-06
F32 = jnp.float32
BF16 = jnp.bfloat16
HIGH = lax.Precision.HIGHEST
MESH = pl.DeviceIdType.MESH


def mm(a, b):
    return jnp.dot(a.astype(BF16), b.astype(BF16), preferred_element_type=F32)


def mm_nt(a, b):
    return lax.dot_general(a, b, (((1,), (1,)), ((), ())), preferred_element_type=F32)


def mm_tn(a, b):
    return lax.dot_general(
        a.astype(BF16), b.astype(BF16), (((0,), (0,)), ((), ())), preferred_element_type=F32
    )


def full(a, b):
    return jnp.dot(a, b, precision=HIGH, preferred_element_type=F32)


def full_nt(a, b):
    return lax.dot_general(
        a, b, (((1,), (1,)), ((), ())), precision=HIGH, preferred_element_type=F32
    )


def silu(x):
    return x / (1.0 + jnp.exp(-x))


def softplus(x):
    return jnp.maximum(x, 0.0) + jnp.log1p(jnp.exp(-jnp.abs(x)))


def unit_lower_inverses(lowers, row, col):
    inverses = []
    for lower in lowers:
        near = jnp.where((row >> 3) == (col >> 3), lower, 0.0)
        inverses.append((near, jnp.where(row == col, 1.0, 0.0) - near))
    squares = [full(d, d) for d, _ in inverses]
    inverses = [x + full(x, s) for (_, x), s in zip(inverses, squares)]
    squares = [full(s, s) for s in squares]
    inverses = [x + full(x, s) for x, s in zip(inverses, squares)]
    for level in (3, 4, 5, 6):
        between = ((row >> (level + 1)) == (col >> (level + 1))) & ((row >> level) != (col >> level))
        parts = [jnp.where(between, lower, 0.0) for lower in lowers]
        parts = [full(p, x) for p, x in zip(parts, inverses)]
        inverses = [x - full(x, p) for p, x in zip(parts, inverses)]
    return inverses


def local_chunk(
    c, q_ref, k_ref, v_ref, strength_ref, decay_ref, extra_ref, rate_ref, maps, from_state, from_values
):
    row = lax.broadcasted_iota(jnp.int32, (CHUNK, CHUNK), 0)
    col = lax.broadcasted_iota(jnp.int32, (CHUNK, CHUNK), 1)
    eye = jnp.where(row == col, 1.0, 0.0)
    lower_ones = jnp.where(row >= col, 1.0, 0.0)
    upper_ones = jnp.where(row <= col, 1.0, 0.0)
    padding = jnp.zeros((6, CHUNK), F32)
    span = pl.ds(pl.multiple_of(c * CHUNK, CHUNK), CHUNK)
    logs = -rate_ref[...] * softplus(decay_ref[:, span].astype(F32)) + extra_ref[:, span]
    beta = 1.0 / (1.0 + jnp.exp(-strength_ref[:, span].astype(F32)))
    logs = jnp.concatenate([logs, padding], axis=0)
    beta = jnp.concatenate([beta, padding], axis=0)
    sums_row = full(logs, upper_ones)
    sums_col = full_nt(lower_ones, logs)
    beta_col = full_nt(eye, beta)
    lowers, scores, rights, keys, queries, closings = [], [], [], [], [], []
    for h in range(2):
        cols = slice(h * HEAD, (h + 1) * HEAD)
        k = k_ref[span, cols]
        q = q_ref[span, cols]
        kf, qf, vf = k.astype(F32), q.astype(F32), v_ref[span, cols].astype(F32)
        squares = kf * kf
        k_col = lax.rsqrt(jnp.sum(squares, axis=1, keepdims=True) + EPSILON)
        k_row = lax.rsqrt(full_nt(jnp.ones((8, HEAD), F32), squares)[0:1] + EPSILON)
        q_col = lax.rsqrt(jnp.sum(qf * qf, axis=1, keepdims=True) + EPSILON) * HEAD ** (-0.5)
        s_col, s_row, b_col = sums_col[:, h : h + 1], sums_row[h : h + 1], beta_col[:, h : h + 1]
        closing = s_row[:, CHUNK - 1 :]
        damping = jnp.exp(jnp.minimum(s_col - s_row, 0.0)) * k_row
        lowers.append(jnp.where(row > col, mm_nt(k, k) * damping * (b_col * k_col), 0.0))
        scores.append(jnp.where(row >= col, mm_nt(q, k) * damping * q_col, 0.0))
        opening = jnp.exp(s_col)
        rights.append(
            jnp.concatenate([kf * (b_col * k_col * opening), vf * b_col], axis=1)
        )
        keys.append(kf * (k_col * jnp.exp(closing - s_col)))
        queries.append(qf * (q_col * opening))
        closings.append(jnp.exp(closing) - 1.0)
    inverses = unit_lower_inverses(lowers, row, col)
    solved = [r + mm(x - eye, r) for x, r in zip(inverses, rights)]
    for h in range(2):
        u = c * 2 + h
        change = mm_tn(keys[h], solved[h])
        maps[u, :, :HEAD] = closings[h] * eye - change[:, :HEAD]
        maps[u, :, HEAD:] = change[:, HEAD:]
        out = mm(scores[h], solved[h])
        from_state[u] = (queries[h] - out[:, :HEAD]).astype(BF16)
        from_values[u] = out[:, HEAD:]


def joined(earlier, later):
    return earlier + later + mm(later[:, :HEAD], earlier)


def carried(state, pair):
    return state + pair[:, HEAD:] + mm(pair[:, :HEAD], state)


A_ROWS = (0, 64)
B_ROWS = (64, 32)


def halves(rows):
    first, count = rows
    return (first, count // 2), (first + count // 2, count // 2)


def sides(rows, offsets, place):
    if len(offsets) == 2:
        return [(place(offsets[0]), rows)], [(place(offsets[1]), rows)]
    low, high = halves(rows)
    return [(place(offsets[0]), low)], [(place(offsets[0]), high)]


class Gather:
    def __init__(self, z, y, c, shard, whole, sems):
        self.z, self.y, self.c, self.shard, self.whole = z, y, c, shard, whole
        self.ring_send, self.sib_send, self.ring_recv, self.sib_recv = sems
        self.used = 0
        self.moves = {}
        self.groups_a = [(0,), (-1, 1), (-2, 2), (-3, 3), (-4,)]
        self.groups_b = [(0,), (-1, 1), (2,)]
        for s in (1, 2, 3):
            for way in (1, -1):
                self.plan("az", s, way, 0, [((-way * s, 0), A_ROWS)])
        for way, blocks in zip((1, -1), sides(A_ROWS, (-4,), lambda o: (o, 0))):
            self.plan("az", 4, way, 0, blocks)
        for g, offsets in enumerate(self.groups_a):
            for way in (1, -1):
                self.plan("ay", (g, 1), way, 1, [((o, -way), A_ROWS) for o in offsets])
            for way, blocks in zip((1, -1), sides(A_ROWS, offsets, lambda o: (o, 2))):
                self.plan("ay", (g, 2), way, 1, blocks)
        for way in (1, -1):
            self.plan("by", 1, way, 1, [((0, -way), B_ROWS)])
        for way, blocks in zip((1, -1), sides(B_ROWS, (2,), lambda o: (0, o))):
            self.plan("by", 2, way, 1, blocks)
        for g, offsets in enumerate(self.groups_b):
            for s in (1, 2, 3):
                for way in (1, -1):
                    self.plan("bz", (g, s), way, 0, [((-way * s, o), B_ROWS) for o in offsets])
            for way, blocks in zip((1, -1), sides(B_ROWS, offsets, lambda o: (4, o))):
                self.plan("bz", (g, 4), way, 0, blocks)

    def plan(self, flow, step, way, axis, blocks):
        entries = []
        for place, rows in blocks:
            entries.append((place, rows, self.used))
            self.used += 1
        self.moves[flow, step, way] = (axis, entries)

    def block(self, place, rows):
        z = (self.z + place[0] + 8) % 8
        y = (self.y + place[1] + 8) % 4
        return self.whole.at[z * 4 + y, self.c, pl.ds(*rows)]

    def copy(self, axis, way, place, rows, sem, src, dst):
        name, size, at = (("sp_0", 8, self.z), ("sp_1", 4, self.y))[axis]
        return pltpu.make_async_remote_copy(
            src_ref=src,
            dst_ref=dst,
            send_sem=self.ring_send,
            recv_sem=self.ring_recv.at[sem],
            device_id={name: (at + way + size) % size},
            device_id_type=MESH,
        )

    def send(self, flow, step):
        for way in (1, -1):
            axis, entries = self.moves[flow, step, way]
            for place, rows, sem in entries:
                shift = (place[0] + way, place[1]) if axis == 0 else (place[0], place[1] + way)
                dst = self.block(shift, rows)
                own = shift[0] % 8 == 0 and shift[1] % 4 == 0
                src = self.shard.at[pl.ds(*rows)] if own else dst
                self.copy(axis, way, place, rows, sem, src, dst).start()

    def receive(self, flow, step):
        for way in (1, -1):
            axis, entries = self.moves[flow, step, way]
            for place, rows, sem in entries:
                block = self.block(place, rows)
                self.copy(axis, way, place, rows, sem, block, block).wait_recv()
                self.across(block, block).start()

    def across(self, src, dst):
        return pltpu.make_async_remote_copy(
            src_ref=src,
            dst_ref=dst,
            send_sem=self.sib_send,
            recv_sem=self.sib_recv,
            device_id={"sp_2": 1 - self.c},
            device_id_type=MESH,
        )

    def start(self):
        self.send("by", 1)
        self.send("az", 1)
        self.send("ay", (0, 1))
        self.send("bz", (0, 1))
        here = self.z * 4 + self.y
        self.across(self.shard, self.whole.at[here, self.c]).start()
        self.whole[here, self.c] = self.shard[...]

    def az(self, s):
        self.receive("az", s)
        if s < 4:
            self.send("az", s + 1)
        self.send("ay", (s, 1))

    def ay(self, g, s):
        self.receive("ay", (g, s))
        if s == 1:
            self.send("ay", (g, 2))

    def by(self, s):
        self.receive("by", s)
        if s == 1:
            self.send("by", 2)
        self.send("bz", (s, 1))

    def bz(self, g, s):
        self.receive("bz", (g, s))
        if s < 4:
            self.send("bz", (g, s + 1))

    def events(self):
        az, ay, by, bz = self.az, self.ay, self.by, self.bz
        return [
            (by, 1), (az, 1), (bz, 0, 1), (ay, 0, 1),
            (by, 2), (az, 2), (bz, 0, 2), (bz, 1, 1),
            (ay, 1, 1), (ay, 0, 2), (az, 3), (bz, 0, 3), (bz, 2, 1), (bz, 1, 2),
            (az, 4), (ay, 1, 2), (ay, 2, 1), (bz, 0, 4), (bz, 2, 2), (bz, 1, 3),
            (ay, 2, 2), (ay, 3, 1), (bz, 2, 3), (bz, 1, 4),
            (ay, 3, 2), (ay, 4, 1), (bz, 2, 4),
            (ay, 4, 2),
        ]

    def finish(self):
        sibling = self.whole.at[:, 1 - self.c]
        self.across(sibling, sibling).wait()
        most = self.whole.at[pl.ds(0, 31), self.c]
        self.copy(0, 1, None, None, 0, most, most).wait_send()


FAR, RIGHT, LEFT, OWN = range(4)
TOK = 96
WIDE = 256


def layer_kernel(
    q_ref,
    k_ref,
    v_ref,
    gate_ref,
    strength_ref,
    decay_ref,
    extra_ref,
    rate_ref,
    gain_ref,
    stream_ref,
    head_ref,
    feed_gain_ref,
    shard,
    result_ref,
    maps,
    from_state,
    from_values,
    totals,
    pair,
    sib,
    chip,
    zin1,
    zin2,
    zin4,
    zout1,
    zout2,
    zout4,
    hin,
    hout,
    mixed,
    mixed_in,
    head_whole,
    residual,
    rows,
    hidden,
    whole,
    far_out,
    relayed,
    outgoing,
    incoming,
    send_sem,
    recv_sem,
    ring_send,
    sib_send,
    ring_recv,
    sib_recv,
):
    z, y, c = lax.axis_index("sp_0"), lax.axis_index("sp_1"), lax.axis_index("sp_2")
    x = lax.axis_index("tp")
    for ref in (zin1, zin2, zin4):
        ref[...] = jnp.zeros_like(ref)
    to_sibling = {"sp_2": 1 - c}
    to_right, to_left, to_far = ({"tp": lax.rem(x + d, 4)} for d in (1, 3, 2))
    barrier = pltpu.get_barrier_semaphore()
    peers = [to_sibling, to_right, to_left, to_far]
    peers += [{"sp_1": lax.rem(y + d, 4)} for d in (1, 2, 3)]
    peers += [{"sp_0": lax.rem(z + d, 8)} for d in (1, 2, 4, 6, 7)]
    for peer in peers:
        pl.semaphore_signal(barrier, inc=1, device_id=peer, device_id_type=MESH)
    pl.semaphore_wait(barrier, len(peers))

    gather = Gather(z, y, c, shard, whole, (ring_send, sib_send, ring_recv, sib_recv))
    gather.start()
    events = iter(gather.events())

    def pump(count):
        for _ in range(count):
            event = next(events, None)
            if event is not None:
                event[0](*event[1:])

    slots = iter(range(64))

    def copy(src, dst, peer):
        slot = next(slots)
        return pltpu.make_async_remote_copy(
            src_ref=src,
            dst_ref=dst,
            send_sem=send_sem.at[slot],
            recv_sem=recv_sem.at[slot],
            device_id=peer,
            device_id_type=MESH,
        )

    half = head_ref.at[pl.ds(pl.multiple_of(c * HEAD, HEAD), HEAD)]
    head_near = [
        copy(half, head_whole.at[LEFT, c], to_right),
        copy(half, head_whole.at[RIGHT, c], to_left),
    ]
    for move in head_near:
        move.start()
    low, high = pl.ds(0, HEAD // 2), pl.ds(HEAD // 2, HEAD // 2)
    head_far = [
        copy(head_whole.at[LEFT, c, low], head_whole.at[FAR, c, low], to_right),
        copy(head_whole.at[RIGHT, c, high], head_whole.at[FAR, c, high], to_left),
    ]
    head_sib = [
        copy(head_whole.at[side, c], head_whole.at[side, c], to_sibling) for side in (FAR, RIGHT, LEFT)
    ]

    for n in range(3):
        local_chunk(
            n,
            q_ref,
            k_ref,
            v_ref,
            strength_ref,
            decay_ref,
            extra_ref,
            rate_ref,
            maps,
            from_state,
            from_values,
        )
        pump(PUMPS[n])
    for h in range(2):
        total = joined(joined(maps[h], maps[2 + h]), maps[4 + h])
        totals[h] = total
        pair[h] = total.astype(BF16)

    to_sib = copy(pair.at[1 - c], sib, to_sibling)
    to_sib.start()
    to_sib.wait()
    own, other = totals[c], sib[...].astype(F32)
    first = jnp.where(c == 0, own, other)
    chip[y] = joined(first, jnp.where(c == 0, other, own)).astype(BF16)
    totals[1] = first

    sends = []
    for d in (1, 2, 3):
        sends.append(copy(chip.at[y], chip.at[y], {"sp_1": lax.rem(y + d, 4)}))
        sends[-1].start()
    pump(PUMPS[3])
    for d in (1, 2, 3):
        sends[d - 1].wait()
    total = chip[0].astype(F32)
    before = jnp.where(y == 0, 0.0, total)
    for s in (1, 2, 3):
        total = joined(total, chip[s].astype(F32))
        if s < 3:
            before = jnp.where(y > s, total, before)

    totals[0] = before
    earlier = jnp.zeros((HEAD, 2 * HEAD), F32)
    for n, (d, out, arrived) in enumerate(((1, zout1, zin1), (2, zout2, zin2), (4, zout4, zin4))):
        out[...] = total[:, (2 * HEAD - out.shape[1]) :].astype(BF16)
        hop = copy(out, arrived, {"sp_0": lax.rem(z + d, 8)})

        @pl.when(z + d < 8)
        def _():
            hop.start()

        pump(PUMPS[4 + n])

        @pl.when(z >= d)
        def _():
            hop.wait_recv()

        came = arrived[...].astype(F32)
        if d < 4:
            earlier = joined(came, earlier)
            total = joined(came, total)
        else:
            state = carried(came, earlier)

        @pl.when(z + d < 8)
        def _():
            hop.wait_send()

        if n == 0:
            for near, far in zip(head_near, head_far):
                near.wait_recv()
                far.start()
            head_sib[2].start()
            head_sib[1].start()
        if n == 2:
            for far in head_far:
                far.wait_recv()
            head_sib[0].start()

    state = carried(state, totals[0])
    later = carried(state, totals[1])
    hout[...] = jnp.where(c == 0, later, state).astype(BF16)
    across = copy(hout, hin, to_sibling)
    across.start()

    def outputs(h, state):
        cols = pl.ds(pl.multiple_of(h * HEAD, HEAD), HEAD)
        for n in range(3):
            u = n * 2 + h
            span = slice(n * CHUNK, (n + 1) * CHUNK)
            out = from_values[u] + mm(from_state[u], state)
            if n < 2:
                state = carried(state, maps[u])
            out = out * lax.rsqrt(jnp.mean(out * out, axis=1, keepdims=True) + EPSILON)
            gated = out * gain_ref[...] * silu(gate_ref[span, cols].astype(F32))
            mixed[span, cols] = gated.astype(BF16)

    outputs(c, jnp.where(c == 0, state, later))
    across.wait()
    outputs(1 - c, hin[...].astype(F32))

    def rows_of(d):
        return pl.ds(pl.multiple_of(lax.rem(x + d, 4) * TOK, TOK), TOK)

    exchange = [
        copy(mixed.at[rows_of(2)], mixed_in.at[FAR], to_far),
        copy(mixed.at[rows_of(1)], mixed_in.at[LEFT], to_right),
        copy(mixed.at[rows_of(3)], mixed_in.at[RIGHT], to_left),
    ]
    for move in exchange:
        move.start()
    pump(PUMPS[7])
    mixed_in[OWN] = mixed[rows_of(0), :]
    for move in head_sib:
        move.wait()
    head_whole[OWN] = head_ref[...].reshape(2, HEAD, -1)
    for move in exchange:
        move.wait()

    def project(n, squares):
        cols = pl.ds(pl.multiple_of(n * WIDE, WIDE), WIDE)
        tile = stream_ref[:, cols].astype(F32)
        for side in range(4):
            matrix = head_whole[side, :, :, cols].reshape(2 * HEAD, WIDE)
            tile = tile + jnp.dot(mixed_in[side], matrix, preferred_element_type=F32)
        residual[:, cols] = tile
        return squares + jnp.sum(tile * tile, axis=1, keepdims=True)

    width = residual.shape[1]
    squares = lax.fori_loop(0, width // WIDE, project, jnp.zeros((TOK, 1), F32))
    scale = lax.rsqrt(squares / width + EPSILON)
    rows[OWN] = (residual[...] * scale * feed_gain_ref[...]).astype(BF16)

    top, bottom = pl.ds(0, TOK // 2), pl.ds(TOK // 2, TOK // 2)
    near = [
        copy(rows.at[OWN, top], rows.at[LEFT, top], to_right),
        copy(rows.at[OWN, bottom], rows.at[RIGHT, bottom], to_left),
        copy(rows.at[OWN, bottom], rows.at[LEFT, bottom], to_right),
        copy(rows.at[OWN, top], rows.at[RIGHT, top], to_left),
    ]
    for move in near:
        move.start()
    relay = [
        copy(rows.at[LEFT, top], rows.at[FAR, top], to_right),
        copy(rows.at[RIGHT, bottom], rows.at[FAR, bottom], to_left),
    ]
    pump(PUMPS[8])
    for move, onward in zip(near, relay):
        move.wait_recv()
        onward.start()
    pump(64)
    gather.finish()
    near[2].wait_recv()
    near[3].wait_recv()
    for move in relay:
        move.wait()
    for move in near + head_near + head_far[:]:
        move.wait_send()

    def gate_up(cols):
        count = cols.size
        block = rows[...].reshape(4 * TOK, width)
        gate = whole[:, :, 0:32, cols].reshape(width, count)
        up = whole[:, :, 64:96, cols].reshape(width, count)
        gate = jnp.dot(block, gate, preferred_element_type=F32)
        up = jnp.dot(block, up, preferred_element_type=F32)
        hidden[:, cols] = (silu(gate) * up).astype(BF16)

    def gate_up_step(n, carry):
        gate_up(pl.ds(pl.multiple_of(n * WIDE, WIDE), WIDE))
        return carry

    units = hidden.shape[1]
    lax.fori_loop(0, units // WIDE, gate_up_step, 0)
    if units % WIDE:
        gate_up(pl.ds(units - units % WIDE, units % WIDE))

    def down(first, count, store):
        def step(n, carry):
            cols = pl.ds(pl.multiple_of(n * WIDE, WIDE), WIDE)
            matrix = whole[pl.ds(n * 4, 4), :, 32:64, :].reshape(WIDE, units)
            store(cols, mm_nt(hidden[first * TOK : (first + count) * TOK], matrix))
            return carry

        lax.fori_loop(0, width // WIDE, step, 0)

    def store_far(cols, tile):
        far_out[:, cols] = tile.astype(BF16)

    def store_near(cols, tile):
        outgoing[:, :, cols] = tile.astype(BF16).reshape(2, TOK, WIDE)

    def store_own(cols, tile):
        residual[:, cols] = residual[:, cols] + tile

    down(FAR, 1, store_far)
    far = [
        copy(far_out.at[top], relayed.at[0], to_right),
        copy(far_out.at[bottom], relayed.at[1], to_left),
    ]
    for move in far:
        move.start()
    down(RIGHT, 2, store_near)
    direct = [
        copy(outgoing.at[0, bottom], incoming.at[0, bottom], to_right),
        copy(outgoing.at[1, top], incoming.at[1, top], to_left),
    ]
    for move in direct:
        move.start()
    for move in far:
        move.wait_recv()
    outgoing[0, top] = (outgoing[0, top].astype(F32) + relayed[0].astype(F32)).astype(BF16)
    outgoing[1, bottom] = (outgoing[1, bottom].astype(F32) + relayed[1].astype(F32)).astype(BF16)
    combined = [
        copy(outgoing.at[0, top], incoming.at[0, top], to_right),
        copy(outgoing.at[1, bottom], incoming.at[1, bottom], to_left),
    ]
    for move in combined:
        move.start()
    down(OWN, 1, store_own)
    for move in direct + combined:
        move.wait()
    for move in far:
        move.wait_send()
    result_ref[...] = (
        residual[...] + (incoming[0].astype(F32) + incoming[1].astype(F32))
    ).astype(BF16)


PUMPS = (1, 2, 2, 1, 3, 3, 4, 2, 2)


def body(
    stream,
    query_projected,
    key_projected,
    value_projected,
    gate_projected,
    strength_logits,
    decay_preactivation,
    extra_log_decay,
    head_decay_rate,
    head_norm_gain,
    head_output_matrix,
    feed_norm_gain,
    gate_matrix,
    up_matrix,
    down_matrix,
):
    width = stream.shape[1]
    units = gate_matrix.shape[1]
    shard = jnp.concatenate([gate_matrix, down_matrix.T, up_matrix], axis=0)
    vmem = pl.BlockSpec(memory_space=pltpu.VMEM)
    pair = (HEAD, 2 * HEAD)
    square = (HEAD, HEAD)
    return pl.pallas_call(
        layer_kernel,
        name="layer",
        out_shape=jax.ShapeDtypeStruct(stream.shape, BF16),
        in_specs=[vmem] * 13,
        out_specs=vmem,
        scratch_shapes=[
            pltpu.VMEM((6, *pair), F32),
            pltpu.VMEM((6, *square), BF16),
            pltpu.VMEM((6, *square), F32),
            pltpu.VMEM((2, *pair), F32),
            pltpu.VMEM((2, *pair), BF16),
            pltpu.VMEM(pair, BF16),
            pltpu.VMEM((4, *pair), BF16),
            pltpu.VMEM(pair, BF16),
            pltpu.VMEM(pair, BF16),
            pltpu.VMEM(square, BF16),
            pltpu.VMEM(pair, BF16),
            pltpu.VMEM(pair, BF16),
            pltpu.VMEM(square, BF16),
            pltpu.VMEM(square, BF16),
            pltpu.VMEM(square, BF16),
            pltpu.VMEM((4 * TOK, 2 * HEAD), BF16),
            pltpu.VMEM((4, TOK, 2 * HEAD), BF16),
            pltpu.VMEM((4, 2, HEAD, width), BF16),
            pltpu.VMEM((TOK, width), F32),
            pltpu.VMEM((4, TOK, width), BF16),
            pltpu.VMEM((4 * TOK, units), BF16),
            pltpu.VMEM((32, 2, 96, units), BF16),
            pltpu.VMEM((TOK, width), BF16),
            pltpu.VMEM((2, TOK // 2, width), BF16),
            pltpu.VMEM((2, TOK, width), BF16),
            pltpu.VMEM((2, TOK, width), BF16),
            pltpu.SemaphoreType.DMA((40,)),
            pltpu.SemaphoreType.DMA((40,)),
            pltpu.SemaphoreType.DMA,
            pltpu.SemaphoreType.DMA,
            pltpu.SemaphoreType.DMA((96,)),
            pltpu.SemaphoreType.DMA,
        ],
        compiler_params=pltpu.CompilerParams(
            collective_id=0, has_side_effects=True, vmem_limit_bytes=60 * 1024 * 1024
        ),
    )(
        query_projected,
        key_projected,
        value_projected,
        gate_projected,
        strength_logits,
        decay_preactivation,
        extra_log_decay,
        head_decay_rate[:, None],
        head_norm_gain[None, :],
        stream,
        head_output_matrix,
        feed_norm_gain[None, :],
        shard,
    )


def solution(mesh):
    torus = Mesh(mesh.devices.reshape(8, 4, 2, mesh.shape["tp"]), ("sp_0", "sp_1", "sp_2", "tp"))
    in_specs = (
        P(SP_TP, None),
        P(SP, "tp"),
        P(SP, "tp"),
        P(SP, "tp"),
        P(SP, "tp"),
        P("tp", SP),
        P("tp", SP),
        P("tp", SP),
        P("tp"),
        P(),
        P("tp", None),
        P(),
        P(SP, "tp"),
        P(SP, "tp"),
        P("tp", SP),
    )
    out_specs = P(SP_TP, None)
    return jax.shard_map(body, mesh=torus, in_specs=in_specs, out_specs=out_specs, check_vma=False)
```

time: 226 us -> 109 us (0.48)
  waiting for transfers between devices: 82.7 us -> 0 us
  Pallas kernels: 29.1 us -> 103 us
  blocking collectives: 70.2 us -> 0 us
  matrix products: 19.3 us -> 0 us
  between operations: 13.5 us -> 0.01 us
  local copies, waits for them, and re-layouts: 7.55 us -> 3.05 us
    all_gather x2 -> x0, waiting for transfers between devices: 82 us -> none  [the longest x1 72.5 us: feed_forward(): down_whole = lax.all_gather(down_matrix, SP, axis=1, tiled=True)]
    pallas_call x1, Pallas kernels: 29.1 us -> 103 us  [body(): pl.pallas_call(layer_kernel, name='layer', out_shape=jax.ShapeDtypeStruct...]
    all_to_all x3 -> x0, blocking collectives: 70.2 us -> none  [the longest x2 48 us: sent_and_summed(): lax.all_to_all(tiles, axis, split_axis=0, concat_axis=0, tiled=True)]
    dot_general x3 -> x0, matrix products: 19.3 us -> none  [the longest x1 11.6 us: feed_forward(): return jnp.dot(hidden, down_whole, preferred_element_type=jnp.float32)]
    unnamed x22 -> x3, local copies, waits for them, and re-layouts: 6.63 us -> 2.42 us
  transfers between devices with their start and end apart: 2 -> 0, of which waited for: 2 -> 0; matrix products, arithmetic and copies ran while one was open for 4% -> 0% of each run, Pallas kernels for 13% -> 0%
where the time goes in v3:
time: 109 us; the launch traced here: 108 us
  Pallas kernels  103 us (94%)
  local copies, waits for them, and re-layouts  3.05 us (3%)
  other arithmetic  1.7 us (2%)
    pallas_call x1, Pallas kernels, body(): pl.pallas_call(layer_kernel, name='layer', out_shape=jax.ShapeDtypeStruct...  103 us
    unnamed x3, local copies, waits for them, and re-layouts  2.42 us

profile of v3, /device:TPU:1, one launch (start us, length us, event | category | flops | bytes accessed | tf_op | source)
XLA Modules:
  0.0 108.1 jit_solution(6266383574230733939)
XLA Ops:
  0.0 0.0 copy-start
  0.0 0.7 copy-done
  0.7 0.6 copy.16.rate_ref
  1.3 1.7 %pad_maximum_fusion.shard = bf16[96,1408]{1,0:T(8,128)(2,1)} fusion(bf16[32,1408]{1,0:T(8,128)(2,1)} %param.28, bf16[32,1408]{1,0:T(8,128)(2,1)} %bitcast.4, bf16[32,1408]{1,0:T(8,128)(2,1)} %param.27), kind=kLoop, calls=%fused_computation | loop fusion | flops 811008 | bytes 540672 | tf_op jit(solution)/shard_map/concatenate | solution.py:633
  3.0 103.3 %layer.1 = bf16[96,2048]{1,0:T(8,128)(2,1)} custom-call(bf16[384,256]{1,0:T(8,128)(2,1)} %q_ref.1, bf16[384,256]{1,0:T(8,128)(2,1)} %k_ref.1, bf16[384,256]{1,0:T(8,128)(2,1)} %v_ref.1, bf16[384,256]{1,0:T(8,128)(2,1)} %gate_ref.1, bf16[2,384]{1,0:T(2,128)(2,1)} %strength_ref.1, bf16[2,384]{1,0:T(2,128)(2,1)} %decay_ref.1, f32[2,384]{1,0:T(2,128)} %extra_ref.1, ...), custom_call_target="tpu_custom_call" | custom-call | tf_op jit(solution)/shard_map/layer/pallas_call | solution.py:637
  106.3 1.8 %copy.18 = bf16[96,2048]{1,0:T(8,128)(2,1)} copy(bf16[96,2048]{1,0:T(8,128)(2,1)} %layer.1) | data formatting | bytes 786432
Async XLA Ops:
  0.0 0.7 copy-start

commit v4 on v3

v4 whole, which is shorter than its diff:
```python
import functools
import jax
import jax.numpy as jnp
from jax import lax
from jax.experimental import pallas as pl
from jax.experimental.pallas import tpu as pltpu
from jax.sharding import Mesh
from jax.sharding import PartitionSpec as P

HEAD = 128
CHUNK = 128
SP = ("sp_0", "sp_1", "sp_2")
SP_TP = ("sp_0", "sp_1", "sp_2", "tp")
EPSILON = 1e-06
F32 = jnp.float32
BF16 = jnp.bfloat16
HIGH = lax.Precision.HIGHEST
MESH = pl.DeviceIdType.MESH


def mm(a, b):
    return jnp.dot(a.astype(BF16), b.astype(BF16), preferred_element_type=F32)


def mm_nt(a, b):
    return lax.dot_general(a, b, (((1,), (1,)), ((), ())), preferred_element_type=F32)


def mm_tn(a, b):
    return lax.dot_general(
        a.astype(BF16), b.astype(BF16), (((0,), (0,)), ((), ())), preferred_element_type=F32
    )


def full(a, b):
    return jnp.dot(a, b, precision=HIGH, preferred_element_type=F32)


def full_nt(a, b):
    return lax.dot_general(
        a, b, (((1,), (1,)), ((), ())), precision=HIGH, preferred_element_type=F32
    )


def silu(x):
    return x / (1.0 + jnp.exp(-x))


def softplus(x):
    return jnp.maximum(x, 0.0) + jnp.log1p(jnp.exp(-jnp.abs(x)))


def halved(a):
    high = a.astype(BF16)
    return high, (a - high.astype(F32)).astype(BF16)


def precise(a, b):
    (ah, al), (bh, bl) = halved(a), halved(b)
    return jnp.dot(
        jnp.concatenate([ah, ah, al], axis=1),
        jnp.concatenate([bh, bl, bh], axis=0),
        preferred_element_type=F32,
    )


def local_part(
    q_ref, k_ref, v_ref, strength_ref, decay_ref, extra_ref, rate_ref, maps, from_state, from_values, pump
):
    row = lax.broadcasted_iota(jnp.int32, (CHUNK, CHUNK), 0)
    col = lax.broadcasted_iota(jnp.int32, (CHUNK, CHUNK), 1)
    eye = jnp.where(row == col, 1.0, 0.0)
    lower_ones = jnp.where(row >= col, 1.0, 0.0)
    upper_ones = jnp.where(row <= col, 1.0, 0.0)
    head = lax.broadcasted_iota(jnp.int32, (2, 1), 0)
    rate = jnp.where(head == 0, rate_ref[0], rate_ref[1])
    logs = -rate * softplus(decay_ref[...].astype(F32)) + extra_ref[...]
    beta = 1.0 / (1.0 + jnp.exp(-strength_ref[...].astype(F32)))
    padding = jnp.zeros((2, CHUNK), F32)
    spans = [slice(n * CHUNK, (n + 1) * CHUNK) for n in range(3)]
    logs = jnp.concatenate([logs[:, s] for s in spans] + [padding], axis=0)
    beta = jnp.concatenate([beta[:, s] for s in spans] + [padding], axis=0)
    sums_row = full(logs, upper_ones)
    sums_col = full_nt(lower_ones, logs)
    beta_col = full_nt(eye, beta)
    lowers, columns = [], []
    for u in range(6):
        span, cols = spans[u // 2], slice((u % 2) * HEAD, (u % 2 + 1) * HEAD)
        k, q = k_ref[span, cols], q_ref[span, cols]
        kf, qf = k.astype(F32), q.astype(F32)
        squares = kf * kf
        k_col = lax.rsqrt(jnp.sum(squares, axis=1, keepdims=True) + EPSILON)
        k_row = lax.rsqrt(full_nt(jnp.ones((8, HEAD), F32), squares)[0:1] + EPSILON)
        q_col = lax.rsqrt(jnp.sum(qf * qf, axis=1, keepdims=True) + EPSILON) * HEAD ** (-0.5)
        s_col, s_row, b_col = sums_col[:, u : u + 1], sums_row[u : u + 1], beta_col[:, u : u + 1]
        damping = jnp.exp(jnp.minimum(s_col - s_row, 0.0)) * k_row
        lowers.append(jnp.where(row > col, mm_nt(k, k) * damping * (b_col * k_col), 0.0))
        from_values[u] = jnp.where(row >= col, mm_nt(q, k) * damping * q_col, 0.0)
        columns.append((k_col, q_col, s_col, b_col, s_row[:, CHUNK - 1 :]))
    pump()
    nears = [jnp.where((row >> 3) == (col >> 3), lower, 0.0) for lower in lowers]
    inverses = [eye - near for near in nears]
    squares = [precise(d, d) for d in nears]
    inverses = [x + precise(x, s) for x, s in zip(inverses, squares)]
    squares = [precise(s, s) for s in squares]
    inverses = [x + precise(x, s) for x, s in zip(inverses, squares)]
    pump()
    for level in (3, 4, 5, 6):
        between = ((row >> (level + 1)) == (col >> (level + 1))) & ((row >> level) != (col >> level))
        parts = [jnp.where(between, lower, 0.0) for lower in lowers]
        parts = [precise(p, x) for p, x in zip(parts, inverses)]
        inverses = [x - precise(x, p) for p, x in zip(parts, inverses)]
        if level in (4, 6):
            pump()
    for u, (k_col, q_col, s_col, b_col, closing) in enumerate(columns):
        span, cols = spans[u // 2], slice((u % 2) * HEAD, (u % 2 + 1) * HEAD)
        kf, qf, vf = (r[span, cols].astype(F32) for r in (k_ref, q_ref, v_ref))
        opening = jnp.exp(s_col)
        right = jnp.concatenate([kf * (b_col * k_col * opening), vf * b_col], axis=1)
        solved = right + mm(inverses[u] - eye, right)
        change = mm_tn(kf * (k_col * jnp.exp(closing - s_col)), solved)
        maps[u, :, :HEAD] = (jnp.exp(closing) - 1.0) * eye - change[:, :HEAD]
        maps[u, :, HEAD:] = change[:, HEAD:]
        out = mm(from_values[u], solved)
        from_state[u] = (qf * (q_col * opening) - out[:, :HEAD]).astype(BF16)
        from_values[u] = out[:, HEAD:]
    pump()


def joined(earlier, later):
    return earlier + later + mm(later[:, :HEAD], earlier)


def carried(state, pair):
    return state + pair[:, HEAD:] + mm(pair[:, :HEAD], state)


GATE_ROWS = (0, 32)
DOWN_ROWS = (32, 32)
UP_ROWS = (64, 32)


def halves(rows):
    first, count = rows
    return (first, count // 2), (first + count // 2, count // 2)


def sides(rows, offsets, place):
    if len(offsets) == 2:
        return [(place(offsets[0]), rows)], [(place(offsets[1]), rows)]
    low, high = halves(rows)
    return [(place(offsets[0]), low)], [(place(offsets[0]), high)]


class Gather:
    def __init__(self, z, y, c, shard, whole, sems):
        self.z, self.y, self.c, self.shard, self.whole = z, y, c, shard, whole
        self.ring_send, self.sib_send, self.ring_recv, self.sib_recv = sems
        self.used = 0
        self.moves = {}
        self.columns = [(0,), (-1, 1), (-2, 2), (-3, 3), (-4,)]
        self.lines = [(0,), (-1, 1), (2,)]
        for flow, rows in (("g", GATE_ROWS), ("d", DOWN_ROWS)):
            for s in (1, 2, 3):
                for way in (1, -1):
                    self.plan(flow + "z", s, way, 0, [((-way * s, 0), rows)])
            for way, blocks in zip((1, -1), sides(rows, (-4,), lambda o: (o, 0))):
                self.plan(flow + "z", 4, way, 0, blocks)
            for n, offsets in enumerate(self.columns):
                for way in (1, -1):
                    self.plan(flow + "y", (n, 1), way, 1, [((o, -way), rows) for o in offsets])
                for way, blocks in zip((1, -1), sides(rows, offsets, lambda o: (o, 2))):
                    self.plan(flow + "y", (n, 2), way, 1, blocks)
        for way in (1, -1):
            self.plan("uy", 1, way, 1, [((0, -way), UP_ROWS)])
        for way, blocks in zip((1, -1), sides(UP_ROWS, (2,), lambda o: (0, o))):
            self.plan("uy", 2, way, 1, blocks)
        for n, offsets in enumerate(self.lines):
            for s in (1, 2, 3):
                for way in (1, -1):
                    self.plan("uz", (n, s), way, 0, [((-way * s, o), UP_ROWS) for o in offsets])
            for way, blocks in zip((1, -1), sides(UP_ROWS, offsets, lambda o: (4, o))):
                self.plan("uz", (n, 4), way, 0, blocks)

    def plan(self, flow, step, way, axis, blocks):
        entries = []
        for place, rows in blocks:
            entries.append((place, rows, self.used))
            self.used += 1
        self.moves[flow, step, way] = (axis, entries)

    def block(self, place, rows):
        z = (self.z + place[0] + 8) % 8
        y = (self.y + place[1] + 8) % 4
        return self.whole.at[z * 4 + y, self.c, pl.ds(*rows)]

    def copy(self, axis, way, place, rows, sem, src, dst):
        name, size, at = (("sp_0", 8, self.z), ("sp_1", 4, self.y))[axis]
        return pltpu.make_async_remote_copy(
            src_ref=src,
            dst_ref=dst,
            send_sem=self.ring_send,
            recv_sem=self.ring_recv.at[sem],
            device_id={name: (at + way + size) % size},
            device_id_type=MESH,
        )

    def send(self, flow, step):
        for way in (1, -1):
            axis, entries = self.moves[flow, step, way]
            for place, rows, sem in entries:
                shift = (place[0] + way, place[1]) if axis == 0 else (place[0], place[1] + way)
                dst = self.block(shift, rows)
                own = shift[0] % 8 == 0 and shift[1] % 4 == 0
                src = self.shard.at[pl.ds(*rows)] if own else dst
                self.copy(axis, way, place, rows, sem, src, dst).start()

    def receive(self, flow, step):
        for way in (1, -1):
            axis, entries = self.moves[flow, step, way]
            for place, rows, sem in entries:
                block = self.block(place, rows)
                self.copy(axis, way, place, rows, sem, block, block).wait_recv()
                self.across(block, block, rows[0] // 32).start()

    def across(self, src, dst, part):
        return pltpu.make_async_remote_copy(
            src_ref=src,
            dst_ref=dst,
            send_sem=self.sib_send,
            recv_sem=self.sib_recv.at[part],
            device_id={"sp_2": 1 - self.c},
            device_id_type=MESH,
        )

    def start(self):
        self.send("uy", 1)
        self.send("gz", 1)
        self.send("gy", (0, 1))
        self.send("uz", (0, 1))
        self.send("dz", 1)
        here = self.z * 4 + self.y
        for part in range(3):
            rows = pl.ds(32 * part, 32)
            self.across(self.shard.at[rows], self.whole.at[here, self.c, rows], part).start()
        self.whole[here, self.c] = self.shard[...]

    def handle(self, kind, *step):
        if kind[1] == "s":
            self.send({"g": "gy", "d": "dy", "u": "uz"}[kind[0]], (step[0], 1))
            return
        self.receive(kind, step if len(step) > 1 else step[0])
        if kind in ("gz", "dz"):
            if step[0] < 4:
                self.send(kind, step[0] + 1)
        elif kind in ("gy", "dy"):
            if step[1] == 1:
                self.send(kind, (step[0], 2))
        elif kind == "uy":
            if step[0] == 1:
                self.send("uy", 2)
        elif step[1] < 4:
            self.send("uz", (step[0], step[1] + 1))

    def from_sibling(self, part):
        block = self.whole.at[:, 1 - self.c, pl.ds(32 * part, 32)]
        self.across(block, block, part).wait_recv()

    def finish(self):
        sibling = self.whole.at[:, 1 - self.c]
        self.across(sibling, sibling, 0).wait_send()
        most = self.whole.at[pl.ds(0, 31), self.c]
        self.copy(0, 1, None, None, 0, most, most).wait_send()


FAR, RIGHT, LEFT, OWN = range(4)
TOK = 96
WIDE = 256


def layer_kernel(
    q_ref,
    k_ref,
    v_ref,
    gate_ref,
    strength_ref,
    decay_ref,
    extra_ref,
    rate_ref,
    gain_ref,
    stream_ref,
    head_ref,
    feed_gain_ref,
    gate_shard,
    up_shard,
    down_shard,
    result_ref,
    maps,
    from_state,
    from_values,
    totals,
    pair,
    sib,
    chip,
    zin1,
    zin2,
    zin4,
    zout1,
    zout2,
    zout4,
    hin,
    hout,
    mixed,
    mixed_in,
    head_whole,
    residual,
    rows,
    hidden,
    shard,
    whole,
    far_out,
    relayed,
    outgoing,
    incoming,
    send_sem,
    recv_sem,
    ring_send,
    sib_send,
    ring_recv,
    sib_recv,
):
    z, y, c = lax.axis_index("sp_0"), lax.axis_index("sp_1"), lax.axis_index("sp_2")
    x = lax.axis_index("tp")
    for ref in (zin1, zin2, zin4):
        ref[...] = jnp.zeros_like(ref)
    to_sibling = {"sp_2": 1 - c}
    to_right, to_left, to_far = ({"tp": lax.rem(x + d, 4)} for d in (1, 3, 2))
    barrier = pltpu.get_barrier_semaphore()
    peers = [to_sibling, to_right, to_left, to_far]
    peers += [{"sp_1": lax.rem(y + d, 4)} for d in (1, 2, 3)]
    peers += [{"sp_0": lax.rem(z + d, 8)} for d in (1, 2, 4, 6, 7)]
    for peer in peers:
        pl.semaphore_signal(barrier, inc=1, device_id=peer, device_id_type=MESH)
    shard[0:32] = gate_shard[...]
    shard[32:64] = down_shard[...].astype(F32).T.astype(BF16)
    shard[64:96] = up_shard[...]
    pl.semaphore_wait(barrier, len(peers))

    gather = Gather(z, y, c, shard, whole, (ring_send, sib_send, ring_recv, sib_recv))
    gather.start()
    schedule = iter(SCHEDULE)

    def pump():
        for event in next(schedule):
            gather.handle(*event)

    slots = iter(range(64))

    def copy(src, dst, peer):
        slot = next(slots)
        return pltpu.make_async_remote_copy(
            src_ref=src,
            dst_ref=dst,
            send_sem=send_sem.at[slot],
            recv_sem=recv_sem.at[slot],
            device_id=peer,
            device_id_type=MESH,
        )

    half = head_ref.at[pl.ds(pl.multiple_of(c * HEAD, HEAD), HEAD)]
    head_near = [
        copy(half, head_whole.at[LEFT, c], to_right),
        copy(half, head_whole.at[RIGHT, c], to_left),
    ]
    for move in head_near:
        move.start()
    low, high = pl.ds(0, HEAD // 2), pl.ds(HEAD // 2, HEAD // 2)
    head_far = [
        copy(head_whole.at[LEFT, c, low], head_whole.at[FAR, c, low], to_right),
        copy(head_whole.at[RIGHT, c, high], head_whole.at[FAR, c, high], to_left),
    ]
    head_sib = [
        copy(head_whole.at[side, c], head_whole.at[side, c], to_sibling) for side in (FAR, RIGHT, LEFT)
    ]

    local_part(
        q_ref,
        k_ref,
        v_ref,
        strength_ref,
        decay_ref,
        extra_ref,
        rate_ref,
        maps,
        from_state,
        from_values,
        pump,
    )
    for h in range(2):
        total = joined(joined(maps[h], maps[2 + h]), maps[4 + h])
        totals[h] = total
        pair[h] = total.astype(BF16)

    to_sib = copy(pair.at[1 - c], sib, to_sibling)
    to_sib.start()
    pump()
    to_sib.wait()
    own, other = totals[c], sib[...].astype(F32)
    first = jnp.where(c == 0, own, other)
    chip[y] = joined(first, jnp.where(c == 0, other, own)).astype(BF16)
    totals[1] = first

    sends = []
    for d in (1, 2, 3):
        sends.append(copy(chip.at[y], chip.at[y], {"sp_1": lax.rem(y + d, 4)}))
        sends[-1].start()
    pump()
    for d in (1, 2, 3):
        sends[d - 1].wait()
    total = chip[0].astype(F32)
    before = jnp.where(y == 0, 0.0, total)
    for s in (1, 2, 3):
        total = joined(total, chip[s].astype(F32))
        if s < 3:
            before = jnp.where(y > s, total, before)

    totals[0] = before
    earlier = jnp.zeros((HEAD, 2 * HEAD), F32)
    for n, (d, out, arrived) in enumerate(((1, zout1, zin1), (2, zout2, zin2), (4, zout4, zin4))):
        out[...] = total[:, (2 * HEAD - out.shape[1]) :].astype(BF16)
        hop = copy(out, arrived, {"sp_0": lax.rem(z + d, 8)})

        @pl.when(z + d < 8)
        def _():
            hop.start()

        pump()

        @pl.when(z >= d)
        def _():
            hop.wait_recv()

        came = arrived[...].astype(F32)
        if d < 4:
            earlier = joined(came, earlier)
            total = joined(came, total)
        else:
            state = carried(came, earlier)

        @pl.when(z + d < 8)
        def _():
            hop.wait_send()

        if n == 0:
            for near, far in zip(head_near, head_far):
                near.wait_recv()
                far.start()
            head_sib[2].start()
            head_sib[1].start()
        if n == 2:
            for far in head_far:
                far.wait_recv()
            head_sib[0].start()

    state = carried(state, totals[0])
    later = carried(state, totals[1])
    hout[...] = jnp.where(c == 0, later, state).astype(BF16)
    across = copy(hout, hin, to_sibling)
    across.start()

    def outputs(h, state):
        cols = pl.ds(pl.multiple_of(h * HEAD, HEAD), HEAD)
        for n in range(3):
            u = n * 2 + h
            span = slice(n * CHUNK, (n + 1) * CHUNK)
            out = from_values[u] + mm(from_state[u], state)
            if n < 2:
                state = carried(state, maps[u])
            out = out * lax.rsqrt(jnp.mean(out * out, axis=1, keepdims=True) + EPSILON)
            gated = out * gain_ref[...] * silu(gate_ref[span, cols].astype(F32))
            mixed[span, cols] = gated.astype(BF16)

    outputs(c, jnp.where(c == 0, state, later))
    pump()
    across.wait()
    outputs(1 - c, hin[...].astype(F32))

    def rows_of(d):
        return pl.ds(pl.multiple_of(lax.rem(x + d, 4) * TOK, TOK), TOK)

    exchange = [
        copy(mixed.at[rows_of(2)], mixed_in.at[FAR], to_far),
        copy(mixed.at[rows_of(1)], mixed_in.at[LEFT], to_right),
        copy(mixed.at[rows_of(3)], mixed_in.at[RIGHT], to_left),
    ]
    for move in exchange:
        move.start()
    pump()
    mixed_in[OWN] = mixed[rows_of(0), :]
    for move in head_sib:
        move.wait()
    head_whole[OWN] = head_ref[...].reshape(2, HEAD, -1)
    for move in exchange:
        move.wait()

    width = residual.shape[1]
    block = jnp.concatenate([mixed_in[side] for side in range(4)], axis=1)
    squares = jnp.zeros((TOK, 1), F32)
    for first in range(0, width, 2 * WIDE):
        cols = slice(first, first + 2 * WIDE)
        matrix = head_whole[:, :, :, cols].reshape(8 * HEAD, 2 * WIDE)
        tile = jnp.dot(block, matrix, preferred_element_type=F32) + stream_ref[:, cols].astype(F32)
        residual[:, cols] = tile
        squares = squares + jnp.sum(tile * tile, axis=1, keepdims=True)
    pump()
    scale = lax.rsqrt(squares / width + EPSILON)
    rows[OWN] = (residual[...] * scale * feed_gain_ref[...]).astype(BF16)

    top, bottom = pl.ds(0, TOK // 2), pl.ds(TOK // 2, TOK // 2)
    near = [
        copy(rows.at[OWN, top], rows.at[LEFT, top], to_right),
        copy(rows.at[OWN, bottom], rows.at[RIGHT, bottom], to_left),
        copy(rows.at[OWN, bottom], rows.at[LEFT, bottom], to_right),
        copy(rows.at[OWN, top], rows.at[RIGHT, top], to_left),
    ]
    for move in near:
        move.start()
    relay = [
        copy(rows.at[LEFT, top], rows.at[FAR, top], to_right),
        copy(rows.at[RIGHT, bottom], rows.at[FAR, bottom], to_left),
    ]
    pump()
    for move, onward in zip(near, relay):
        move.wait_recv()
        onward.start()
    pump()
    gather.from_sibling(0)
    gather.from_sibling(2)
    near[2].wait_recv()
    near[3].wait_recv()

    def gate_up(first, count, cols):
        tile = cols.stop - cols.start
        block = rows[first : first + count].reshape(count * TOK, width)
        gate = whole[:, :, 0:32, cols].reshape(width, tile)
        up = whole[:, :, 64:96, cols].reshape(width, tile)
        gate = jnp.dot(block, gate, preferred_element_type=F32)
        up = jnp.dot(block, up, preferred_element_type=F32)
        hidden[first * TOK : (first + count) * TOK, cols] = (silu(gate) * up).astype(BF16)

    units = hidden.shape[1]
    tiles = [slice(n, min(n + WIDE, units)) for n in range(0, units, WIDE)]
    for cols in tiles:
        gate_up(RIGHT, 3, cols)
        pump()
    for move in relay:
        move.wait()
    for cols in tiles:
        gate_up(FAR, 1, cols)
    pump()
    gather.from_sibling(1)

    def down(first, count, store, part=(0, 2)):
        def step(n, carry):
            cols = pl.ds(pl.multiple_of(n * WIDE, WIDE), WIDE)
            matrix = whole[pl.ds(n * 4, 4), :, 32:64, :].reshape(WIDE, units)
            store(cols, mm_nt(hidden[first * TOK : (first + count) * TOK], matrix))
            return carry

        steps = width // WIDE // 2
        lax.fori_loop(part[0] * steps, part[1] * steps, step, 0)

    def store_far(cols, tile):
        far_out[:, cols] = tile.astype(BF16)

    def store_near(cols, tile):
        outgoing[:, :, cols] = tile.astype(BF16).reshape(2, TOK, WIDE)

    def store_own(cols, tile):
        residual[:, cols] = residual[:, cols] + tile

    far, direct, combined = [], [], []
    for part in range(2):
        cols = pl.ds(part * width // 2, width // 2)
        down(FAR, 1, store_far, (part, part + 1))
        far += [
            copy(far_out.at[top, cols], relayed.at[0, :, cols], to_right),
            copy(far_out.at[bottom, cols], relayed.at[1, :, cols], to_left),
        ]
        for move in far[-2:]:
            move.start()
    for part in range(2):
        cols = pl.ds(part * width // 2, width // 2)
        down(RIGHT, 2, store_near, (part, part + 1))
        direct += [
            copy(outgoing.at[0, bottom, cols], incoming.at[0, bottom, cols], to_right),
            copy(outgoing.at[1, top, cols], incoming.at[1, top, cols], to_left),
        ]
        for move in direct[-2:]:
            move.start()
    for part in range(2):
        cols = pl.ds(part * width // 2, width // 2)
        for side, rows_half in ((0, top), (1, bottom)):
            far[2 * part + side].wait_recv()
            mine = outgoing[side, rows_half, cols].astype(F32)
            outgoing[side, rows_half, cols] = (mine + relayed[side, :, cols].astype(F32)).astype(BF16)
        combined += [
            copy(outgoing.at[0, top, cols], incoming.at[0, top, cols], to_right),
            copy(outgoing.at[1, bottom, cols], incoming.at[1, bottom, cols], to_left),
        ]
        for move in combined[-2:]:
            move.start()
    down(OWN, 1, store_own)
    for move in direct + combined:
        move.wait()
    for move in far:
        move.wait_send()
    result_ref[...] = (
        residual[...] + (incoming[0].astype(F32) + incoming[1].astype(F32))
    ).astype(BF16)
    for move in near + head_near + head_far:
        move.wait_send()
    gather.finish()


SCHEDULE = (
    (("ds", 0),),
    (),
    (),
    (),
    (("uy", 1), ("gz", 1),),
    (("gy", 0, 1), ("uz", 0, 1),),
    (("gs", 1), ("us", 1), ("uy", 2), ("dy", 0, 1), ("gz", 2), ("gs", 2), ("gy", 0, 2),),
    (("dz", 1), ("gz", 3), ("gs", 3), ("gy", 1, 1),),
    (("us", 2), ("uz", 0, 2), ("gz", 4), ("gs", 4), ("gy", 2, 1), ("dy", 0, 2),),
    (("uz", 1, 1), ("uz", 2, 1), ("dz", 2), ("ds", 1), ("gy", 1, 2),),
    (("uz", 0, 3), ("gy", 3, 1),),
    (("gy", 2, 2), ("ds", 2), ("dz", 3), ("uz", 1, 2), ("uz", 2, 2),),
    (("uz", 0, 4), ("ds", 3), ("gy", 4, 1), ("gy", 3, 2),),
    (("dz", 4), ("ds", 4), ("uz", 1, 3), ("uz", 2, 3), ("dy", 1, 1),),
    (("dy", 2, 1), ("dy", 3, 1), ("uz", 1, 4), ("uz", 2, 4), ("gy", 4, 2), ("dy", 4, 1),),
    (),
    (),
    (("dy", 1, 2),),
    (),
    (("dy", 2, 2),),
    (("dy", 3, 2),),
    (("dy", 4, 2),),
)


def body(
    stream,
    query_projected,
    key_projected,
    value_projected,
    gate_projected,
    strength_logits,
    decay_preactivation,
    extra_log_decay,
    head_decay_rate,
    head_norm_gain,
    head_output_matrix,
    feed_norm_gain,
    gate_matrix,
    up_matrix,
    down_matrix,
):
    width = stream.shape[1]
    units = gate_matrix.shape[1]
    vmem = pl.BlockSpec(memory_space=pltpu.VMEM)
    pair = (HEAD, 2 * HEAD)
    square = (HEAD, HEAD)
    return pl.pallas_call(
        layer_kernel,
        name="layer",
        out_shape=jax.ShapeDtypeStruct(stream.shape, BF16),
        in_specs=[vmem] * 7 + [pl.BlockSpec(memory_space=pltpu.SMEM)] + [vmem] * 7,
        out_specs=vmem,
        scratch_shapes=[
            pltpu.VMEM((6, *pair), F32),
            pltpu.VMEM((6, *square), BF16),
            pltpu.VMEM((6, *square), F32),
            pltpu.VMEM((2, *pair), F32),
            pltpu.VMEM((2, *pair), BF16),
            pltpu.VMEM(pair, BF16),
            pltpu.VMEM((4, *pair), BF16),
            pltpu.VMEM(pair, BF16),
            pltpu.VMEM(pair, BF16),
            pltpu.VMEM(square, BF16),
            pltpu.VMEM(pair, BF16),
            pltpu.VMEM(pair, BF16),
            pltpu.VMEM(square, BF16),
            pltpu.VMEM(square, BF16),
            pltpu.VMEM(square, BF16),
            pltpu.VMEM((4 * TOK, 2 * HEAD), BF16),
            pltpu.VMEM((4, TOK, 2 * HEAD), BF16),
            pltpu.VMEM((4, 2, HEAD, width), BF16),
            pltpu.VMEM((TOK, width), F32),
            pltpu.VMEM((4, TOK, width), BF16),
            pltpu.VMEM((4 * TOK, units), BF16),
            pltpu.VMEM((96, units), BF16),
            pltpu.VMEM((32, 2, 96, units), BF16),
            pltpu.VMEM((TOK, width), BF16),
            pltpu.VMEM((2, TOK // 2, width), BF16),
            pltpu.VMEM((2, TOK, width), BF16),
            pltpu.VMEM((2, TOK, width), BF16),
            pltpu.SemaphoreType.DMA((48,)),
            pltpu.SemaphoreType.DMA((48,)),
            pltpu.SemaphoreType.DMA,
            pltpu.SemaphoreType.DMA,
            pltpu.SemaphoreType.DMA((104,)),
            pltpu.SemaphoreType.DMA((3,)),
        ],
        compiler_params=pltpu.CompilerParams(
            collective_id=0, has_side_effects=True, vmem_limit_bytes=60 * 1024 * 1024
        ),
    )(
        query_projected,
        key_projected,
        value_projected,
        gate_projected,
        strength_logits,
        decay_preactivation,
        extra_log_decay,
        head_decay_rate,
        head_norm_gain[None, :],
        stream,
        head_output_matrix,
        feed_norm_gain[None, :],
        gate_matrix,
        up_matrix,
        down_matrix,
    )


def solution(mesh):
    torus = Mesh(mesh.devices.reshape(8, 4, 2, mesh.shape["tp"]), ("sp_0", "sp_1", "sp_2", "tp"))
    in_specs = (
        P(SP_TP, None),
        P(SP, "tp"),
        P(SP, "tp"),
        P(SP, "tp"),
        P(SP, "tp"),
        P("tp", SP),
        P("tp", SP),
        P("tp", SP),
        P("tp"),
        P(),
        P("tp", None),
        P(),
        P(SP, "tp"),
        P(SP, "tp"),
        P("tp", SP),
    )
    out_specs = P(SP_TP, None)
    return jax.shard_map(body, mesh=torus, in_specs=in_specs, out_specs=out_specs, check_vma=False)
```

time: 109 us -> 92.4 us (0.85)
  Pallas kernels: 103 us -> 88.7 us
  other arithmetic: 1.7 us -> 0 us
    pallas_call x1, Pallas kernels: 103 us -> 88.7 us  [body(): pl.pallas_call(layer_kernel, name='layer', out_shape=jax.ShapeDtypeStruct...]
    concatenate x1 -> x0, other arithmetic: 1.7 us -> none  [body(): shard = jnp.concatenate([gate_matrix, down_matrix.T, up_matrix], axis=0)]
    unnamed x3 -> x2, local copies, waits for them, and re-layouts: 2.42 us -> 3.57 us
where the time goes in v4:
time: 92.4 us; the launch traced here: 92.3 us
  Pallas kernels  88.7 us (96%)
  local copies, waits for them, and re-layouts  3.57 us (4%)
    pallas_call x1, Pallas kernels, body(): pl.pallas_call(layer_kernel, name='layer', out_shape=jax.ShapeDtypeStruct...  88.7 us
    unnamed x2, local copies, waits for them, and re-layouts  3.57 us

profile of v4, /device:TPU:1, one launch (start us, length us, event | category | flops | bytes accessed | tf_op | source)
XLA Modules:
  0.0 92.3 jit_solution(13958291197996882461)
XLA Ops:
  0.0 1.8 %copy.16.down_shard = bf16[1408,32]{1,0:T(8,128)(2,1)} copy(bf16[1408,32]{0,1:T(8,128)(2,1)} %param.29) | data formatting | bytes 180224 | tf_op args[14]
  1.8 88.7 %layer.1 = bf16[96,2048]{1,0:T(8,128)(2,1)} custom-call(bf16[384,256]{1,0:T(8,128)(2,1)} %q_ref.1, bf16[384,256]{1,0:T(8,128)(2,1)} %k_ref.1, bf16[384,256]{1,0:T(8,128)(2,1)} %v_ref.1, bf16[384,256]{1,0:T(8,128)(2,1)} %gate_ref.1, bf16[2,384]{1,0:T(2,128)(2,1)} %strength_ref.1, bf16[2,384]{1,0:T(2,128)(2,1)} %decay_ref.1, f32[2,384]{1,0:T(2,128)} %extra_ref.1, ...), custom_call_target="tpu_custom_call" | custom-call | tf_op jit(solution)/shard_map/layer/pallas_call | solution.py:674
  90.5 1.8 %copy.18 = bf16[96,2048]{1,0:T(8,128)(2,1)} copy(bf16[96,2048]{1,0:T(8,128)(2,1)} %layer.1) | data formatting | bytes 786432

commit v5 on v4

--- a/solution.py
+++ b/solution.py
@@ -65,7 +65,7 @@
 
 
 def local_part(
-    q_ref, k_ref, v_ref, strength_ref, decay_ref, extra_ref, rate_ref, maps, from_state, from_values, pump
+    q_ref, k_ref, v_ref, strength_ref, decay_ref, extra_ref, rate_ref, maps, from_state, from_values, begin, pump
 ):
     row = lax.broadcasted_iota(jnp.int32, (CHUNK, CHUNK), 0)
     col = lax.broadcasted_iota(jnp.int32, (CHUNK, CHUNK), 1)
@@ -97,6 +97,7 @@
         lowers.append(jnp.where(row > col, mm_nt(k, k) * damping * (b_col * k_col), 0.0))
         from_values[u] = jnp.where(row >= col, mm_nt(q, k) * damping * q_col, 0.0)
         columns.append((k_col, q_col, s_col, b_col, s_row[:, CHUNK - 1 :]))
+    begin()
     pump()
     nears = [jnp.where((row >> 3) == (col >> 3), lower, 0.0) for lower in lowers]
     inverses = [eye - near for near in nears]
@@ -135,13 +136,8 @@
     return state + pair[:, HEAD:] + mm(pair[:, :HEAD], state)
 
 
-GATE_ROWS = (0, 32)
-DOWN_ROWS = (32, 32)
-UP_ROWS = (64, 32)
-
-
-def halves(rows):
-    first, count = rows
+def halves(region):
+    first, count = region
     return (first, count // 2), (first + count // 2, count // 2)
 
 
@@ -159,8 +155,9 @@
         self.used = 0
         self.moves = {}
         self.columns = [(0,), (-1, 1), (-2, 2), (-3, 3), (-4,)]
-        self.lines = [(0,), (-1, 1), (2,)]
-        for flow, rows in (("g", GATE_ROWS), ("d", DOWN_ROWS)):
+        self.lines = [(0,), (-1,), (1,), (2,)]
+        gate, down, up = (0, 32), (32, 32), (64, 32)
+        for flow, rows in (("g", gate), ("d", down)):
             for s in (1, 2, 3):
                 for way in (1, -1):
                     self.plan(flow + "z", s, way, 0, [((-way * s, 0), rows)])
@@ -171,16 +168,17 @@
                     self.plan(flow + "y", (n, 1), way, 1, [((o, -way), rows) for o in offsets])
                 for way, blocks in zip((1, -1), sides(rows, offsets, lambda o: (o, 2))):
                     self.plan(flow + "y", (n, 2), way, 1, blocks)
-        for way in (1, -1):
-            self.plan("uy", 1, way, 1, [((0, -way), UP_ROWS)])
-        for way, blocks in zip((1, -1), sides(UP_ROWS, (2,), lambda o: (0, o))):
-            self.plan("uy", 2, way, 1, blocks)
-        for n, offsets in enumerate(self.lines):
-            for s in (1, 2, 3):
-                for way in (1, -1):
-                    self.plan("uz", (n, s), way, 0, [((-way * s, o), UP_ROWS) for o in offsets])
-            for way, blocks in zip((1, -1), sides(UP_ROWS, offsets, lambda o: (4, o))):
-                self.plan("uz", (n, 4), way, 0, blocks)
+        for flow, rows in (("u", up),):
+            for way in (1, -1):
+                self.plan(flow + "y", 1, way, 1, [((0, -way), rows)])
+            for way, blocks in zip((1, -1), sides(rows, (2,), lambda o: (0, o))):
+                self.plan(flow + "y", 2, way, 1, blocks)
+            for n, offsets in enumerate(self.lines):
+                for s in (1, 2, 3):
+                    for way in (1, -1):
+                        self.plan(flow + "z", (n, s), way, 0, [((-way * s, o), rows) for o in offsets])
+                for way, blocks in zip((1, -1), sides(rows, offsets, lambda o: (4, o))):
+                    self.plan(flow + "z", (n, 4), way, 0, blocks)
 
     def plan(self, flow, step, way, axis, blocks):
         entries = []
@@ -258,9 +256,9 @@
                 self.send(kind, (step[0], 2))
         elif kind == "uy":
             if step[0] == 1:
-                self.send("uy", 2)
+                self.send(kind, 2)
         elif step[1] < 4:
-            self.send("uz", (step[0], step[1] + 1))
+            self.send(kind, (step[0], step[1] + 1))
 
     def from_sibling(self, part):
         block = self.whole.at[:, 1 - self.c, pl.ds(32 * part, 32)]
@@ -279,6 +277,22 @@
 
 
 def layer_kernel(
+    q_hbm,
+    k_hbm,
+    v_hbm,
+    gate_hbm,
+    strength_hbm,
+    decay_hbm,
+    extra_hbm,
+    rate_ref,
+    gain_ref,
+    stream_hbm,
+    head_hbm,
+    feed_gain_ref,
+    gate_shard,
+    up_shard,
+    down_shard,
+    result_ref,
     q_ref,
     k_ref,
     v_ref,
@@ -286,15 +300,9 @@
     strength_ref,
     decay_ref,
     extra_ref,
-    rate_ref,
-    gain_ref,
     stream_ref,
     head_ref,
-    feed_gain_ref,
-    gate_shard,
-    up_shard,
-    down_shard,
-    result_ref,
+    load_sem,
     maps,
     from_state,
     from_values,
@@ -315,6 +323,7 @@
     head_whole,
     residual,
     rows,
+    gated,
     hidden,
     shard,
     whole,
@@ -331,23 +340,42 @@
 ):
     z, y, c = lax.axis_index("sp_0"), lax.axis_index("sp_1"), lax.axis_index("sp_2")
     x = lax.axis_index("tp")
+    to_sibling = {"sp_2": 1 - c}
+    to_right, to_left, to_far = ({"tp": lax.rem(x + d, 4)} for d in (1, 3, 2))
     for ref in (zin1, zin2, zin4):
         ref[...] = jnp.zeros_like(ref)
-    to_sibling = {"sp_2": 1 - c}
-    to_right, to_left, to_far = ({"tp": lax.rem(x + d, 4)} for d in (1, 3, 2))
+    loads = {}
+    pairs = (
+        ("shards", gate_shard, shard.at[pl.ds(0, 32)]),
+        ("shards", down_shard, shard.at[pl.ds(32, 32)]),
+        ("shards", up_shard, shard.at[pl.ds(64, 32)]),
+        ("local", strength_hbm, strength_ref),
+        ("local", decay_hbm, decay_ref),
+        ("local", extra_hbm, extra_ref),
+        ("local", k_hbm, k_ref),
+        ("local", q_hbm, q_ref),
+        ("local", v_hbm, v_ref),
+        ("shards", head_hbm, head_ref),
+        ("late", gate_hbm, gate_ref),
+        ("late", stream_hbm, stream_ref),
+    )
+
+    def arrived_loads(group):
+        for load in loads[group]:
+            load.wait()
+
     barrier = pltpu.get_barrier_semaphore()
     peers = [to_sibling, to_right, to_left, to_far]
     peers += [{"sp_1": lax.rem(y + d, 4)} for d in (1, 2, 3)]
     peers += [{"sp_0": lax.rem(z + d, 8)} for d in (1, 2, 4, 6, 7)]
     for peer in peers:
         pl.semaphore_signal(barrier, inc=1, device_id=peer, device_id_type=MESH)
-    shard[0:32] = gate_shard[...]
-    shard[32:64] = down_shard[...].astype(F32).T.astype(BF16)
-    shard[64:96] = up_shard[...]
-    pl.semaphore_wait(barrier, len(peers))
+    for n, (group, src, dst) in enumerate(pairs):
+        load = pltpu.make_async_copy(src, dst, load_sem.at[n])
+        load.start()
+        loads.setdefault(group, []).append(load)
 
     gather = Gather(z, y, c, shard, whole, (ring_send, sib_send, ring_recv, sib_recv))
-    gather.start()
     schedule = iter(SCHEDULE)
 
     def pump():
@@ -372,8 +400,6 @@
         copy(half, head_whole.at[LEFT, c], to_right),
         copy(half, head_whole.at[RIGHT, c], to_left),
     ]
-    for move in head_near:
-        move.start()
     low, high = pl.ds(0, HEAD // 2), pl.ds(HEAD // 2, HEAD // 2)
     head_far = [
         copy(head_whole.at[LEFT, c, low], head_whole.at[FAR, c, low], to_right),
@@ -383,6 +409,14 @@
         copy(head_whole.at[side, c], head_whole.at[side, c], to_sibling) for side in (FAR, RIGHT, LEFT)
     ]
 
+    def begin():
+        arrived_loads("shards")
+        pl.semaphore_wait(barrier, len(peers))
+        gather.start()
+        for move in head_near:
+            move.start()
+
+    arrived_loads("local")
     local_part(
         q_ref,
         k_ref,
@@ -394,6 +428,7 @@
         maps,
         from_state,
         from_values,
+        begin,
         pump,
     )
     for h in range(2):
@@ -462,6 +497,7 @@
                 far.wait_recv()
             head_sib[0].start()
 
+    arrived_loads("late")
     state = carried(state, totals[0])
     later = carried(state, totals[1])
     hout[...] = jnp.where(c == 0, later, state).astype(BF16)
@@ -535,28 +571,30 @@
         onward.start()
     pump()
     gather.from_sibling(0)
-    gather.from_sibling(2)
+
+    units = hidden.shape[1]
+    tiles = [slice(n, min(n + WIDE, units)) for n in range(0, units, WIDE)]
+
+    def times(first, count, part, cols):
+        matrix = whole[:, :, 32 * part : 32 * part + 32, cols].reshape(width, cols.stop - cols.start)
+        block = rows[first : first + count].reshape(count * TOK, width)
+        return jnp.dot(block, matrix, preferred_element_type=F32)
+
     near[2].wait_recv()
     near[3].wait_recv()
-
-    def gate_up(first, count, cols):
-        tile = cols.stop - cols.start
-        block = rows[first : first + count].reshape(count * TOK, width)
-        gate = whole[:, :, 0:32, cols].reshape(width, tile)
-        up = whole[:, :, 64:96, cols].reshape(width, tile)
-        gate = jnp.dot(block, gate, preferred_element_type=F32)
-        up = jnp.dot(block, up, preferred_element_type=F32)
-        hidden[first * TOK : (first + count) * TOK, cols] = (silu(gate) * up).astype(BF16)
-
-    units = hidden.shape[1]
-    tiles = [slice(n, min(n + WIDE, units)) for n in range(0, units, WIDE)]
     for cols in tiles:
-        gate_up(RIGHT, 3, cols)
+        gated[:, cols] = silu(times(RIGHT, 3, 0, cols))
+        pump()
+    pump()
+    gather.from_sibling(2)
+    for cols in tiles:
+        hidden[TOK:, cols] = (gated[:, cols] * times(RIGHT, 3, 2, cols)).astype(BF16)
         pump()
     for move in relay:
         move.wait()
     for cols in tiles:
-        gate_up(FAR, 1, cols)
+        far_gate = silu(times(FAR, 1, 0, cols))
+        hidden[:TOK, cols] = (far_gate * times(FAR, 1, 2, cols)).astype(BF16)
     pump()
     gather.from_sibling(1)
 
@@ -628,22 +666,29 @@
     (),
     (),
     (),
-    (("uy", 1), ("gz", 1),),
-    (("gy", 0, 1), ("uz", 0, 1),),
-    (("gs", 1), ("us", 1), ("uy", 2), ("dy", 0, 1), ("gz", 2), ("gs", 2), ("gy", 0, 2),),
-    (("dz", 1), ("gz", 3), ("gs", 3), ("gy", 1, 1),),
-    (("us", 2), ("uz", 0, 2), ("gz", 4), ("gs", 4), ("gy", 2, 1), ("dy", 0, 2),),
-    (("uz", 1, 1), ("uz", 2, 1), ("dz", 2), ("ds", 1), ("gy", 1, 2),),
-    (("uz", 0, 3), ("gy", 3, 1),),
-    (("gy", 2, 2), ("ds", 2), ("dz", 3), ("uz", 1, 2), ("uz", 2, 2),),
-    (("uz", 0, 4), ("ds", 3), ("gy", 4, 1), ("gy", 3, 2),),
-    (("dz", 4), ("ds", 4), ("uz", 1, 3), ("uz", 2, 3), ("dy", 1, 1),),
-    (("dy", 2, 1), ("dy", 3, 1), ("uz", 1, 4), ("uz", 2, 4), ("gy", 4, 2), ("dy", 4, 1),),
-    (),
-    (),
-    (("dy", 1, 2),),
+    (),
+    (),
+    (("uy", 1), ("gz", 1), ("gs", 1), ("gy", 0, 1), ("uz", 0, 1), ("us", 1),),
+    (("gz", 2), ("gs", 2), ("uy", 2), ("dy", 0, 1), ("us", 2),),
+    (("gz", 3), ("gs", 3), ("gy", 0, 2), ("gy", 1, 1), ("us", 3), ("dz", 1),),
+    (("uz", 0, 2), ("uz", 1, 1), ("uz", 2, 1), ("gz", 4), ("gs", 4), ("dy", 0, 2), ("ds", 1), ("gy", 2, 1),),
+    (("uz", 3, 1), ("dz", 2), ("gy", 3, 1),),
+    (("gy", 1, 2), ("ds", 2),),
+    (("uz", 3, 2), ("uz", 0, 3), ("uz", 1, 2), ("uz", 2, 2), ("gy", 4, 1),),
+    (("gy", 2, 2), ("gy", 3, 2), ("dy", 1, 1), ("dz", 3), ("ds", 3),),
+    (("uz", 0, 4), ("uz", 1, 3), ("uz", 3, 3), ("uz", 2, 3), ("gy", 4, 2), ("dy", 2, 1), ("dz", 4), ("ds", 4),),
+    (("dy", 3, 1),),
+    (),
+    (),
+    (),
+    (),
+    (),
+    (("uz", 1, 4), ("uz", 2, 4), ("uz", 3, 4),),
+    (("dy", 1, 2), ("dy", 4, 1),),
+    (),
     (),
     (("dy", 2, 2),),
+    (),
     (("dy", 3, 2),),
     (("dy", 4, 2),),
 )
@@ -669,15 +714,24 @@
     width = stream.shape[1]
     units = gate_matrix.shape[1]
     vmem = pl.BlockSpec(memory_space=pltpu.VMEM)
+    hbm = pl.BlockSpec(memory_space=pl.ANY)
+    tokens = query_projected.shape[0]
     pair = (HEAD, 2 * HEAD)
     square = (HEAD, HEAD)
     return pl.pallas_call(
         layer_kernel,
         name="layer",
         out_shape=jax.ShapeDtypeStruct(stream.shape, BF16),
-        in_specs=[vmem] * 7 + [pl.BlockSpec(memory_space=pltpu.SMEM)] + [vmem] * 7,
+        in_specs=[hbm] * 7 + [pl.BlockSpec(memory_space=pltpu.SMEM), vmem] + [hbm] * 2 + [vmem] + [hbm] * 3,
         out_specs=vmem,
         scratch_shapes=[
+            *[pltpu.VMEM((tokens, 2 * HEAD), BF16)] * 4,
+            pltpu.VMEM((2, tokens), BF16),
+            pltpu.VMEM((2, tokens), BF16),
+            pltpu.VMEM((2, tokens), F32),
+            pltpu.VMEM((TOK, width), BF16),
+            pltpu.VMEM((2 * HEAD, width), BF16),
+            pltpu.SemaphoreType.DMA((12,)),
             pltpu.VMEM((6, *pair), F32),
             pltpu.VMEM((6, *square), BF16),
             pltpu.VMEM((6, *square), F32),
@@ -698,6 +752,7 @@
             pltpu.VMEM((4, 2, HEAD, width), BF16),
             pltpu.VMEM((TOK, width), F32),
             pltpu.VMEM((4, TOK, width), BF16),
+            pltpu.VMEM((3 * TOK, units), F32),
             pltpu.VMEM((4 * TOK, units), BF16),
             pltpu.VMEM((96, units), BF16),
             pltpu.VMEM((32, 2, 96, units), BF16),
@@ -709,7 +764,7 @@
             pltpu.SemaphoreType.DMA((48,)),
             pltpu.SemaphoreType.DMA,
             pltpu.SemaphoreType.DMA,
-            pltpu.SemaphoreType.DMA((104,)),
+            pltpu.SemaphoreType.DMA((144,)),
             pltpu.SemaphoreType.DMA((3,)),
         ],
         compiler_params=pltpu.CompilerParams(
@@ -730,7 +785,7 @@
         feed_norm_gain[None, :],
         gate_matrix,
         up_matrix,
-        down_matrix,
+        down_matrix.T,
     )
 
 

time: 92.4 us -> 91.6 us (level)
  local copies, waits for them, and re-layouts: 3.57 us -> 1.77 us
    unnamed x2 -> x1, local copies, waits for them, and re-layouts: 3.57 us -> 1.77 us
    pallas_call x1, Pallas kernels: 88.7 us -> 89.6 us  [body(): pl.pallas_call(layer_kernel, name='layer', out_shape=jax.ShapeDtypeStruct...]
where the time goes in v5:
time: 91.6 us; the launch traced here: 91.4 us
  Pallas kernels  89.6 us (98%)
  local copies, waits for them, and re-layouts  1.77 us (2%)
    pallas_call x1, Pallas kernels, body(): pl.pallas_call(layer_kernel, name='layer', out_shape=jax.ShapeDtypeStruct...  89.6 us

profile of v5, /device:TPU:1, one launch (start us, length us, event | category | flops | bytes accessed | tf_op | source)
XLA Modules:
  0.0 91.4 jit_solution(5673310061016491017)
XLA Ops:
  0.0 89.6 %layer.1 = bf16[96,2048]{1,0:T(8,128)(2,1)} custom-call(bf16[384,256]{1,0:T(8,128)(2,1)} %q_hbm.1, bf16[384,256]{1,0:T(8,128)(2,1)} %k_hbm.1, bf16[384,256]{1,0:T(8,128)(2,1)} %v_hbm.1, bf16[384,256]{1,0:T(8,128)(2,1)} %gate_hbm.1, bf16[2,384]{1,0:T(2,128)(2,1)} %strength_hbm.1, bf16[2,384]{1,0:T(2,128)(2,1)} %decay_hbm.1, f32[2,384]{1,0:T(2,128)} %extra_hbm.1, ...), custom_call_target="tpu_custom_call" | custom-call | tf_op jit(solution)/shard_map/layer/pallas_call | solution.py:721
  89.6 1.8 %copy.17 = bf16[96,2048]{1,0:T(8,128)(2,1)} copy(bf16[96,2048]{1,0:T(8,128)(2,1)} %layer.1) | data formatting | bytes 786432
